TPU v7x, 32 devices: a whole 2x2x4 slice. The times are simulated.
32 devices in a mesh: grp: 2 (over y), sp: 4 (over z), tp: 4 (over x, core).
Axes of the slice: x: 2, y: 2, z: 4, core: 2. Of those that a mesh axis runs over, the one named last changes fastest.
Arguments:
- tokens: bfloat16 [1280, 2048], P(('grp', 'sp')), parts along dimension 0, may hold values from -6 to 6
- norm_gain: float32 [2048], replicated, may hold values from 0.6 to 5
- query_weight: bfloat16 [2048, 2048], P('sp', 'tp')
- key_weight: bfloat16 [2048, 512], P('sp', 'tp')
- value_weight: bfloat16 [2048, 512], P('sp', 'tp'), may hold values from -0.125 to 0.125
- map_lambda: float32 [16], P('tp'), may hold values from 0.3 to 0.8
- head_gain: float32 [16, 128], P('tp'), may hold values from 0.1 to 1.9
- attn_out_weight: bfloat16 [2048, 2048], P('tp', 'sp'), may hold values from -0.125 to 0.125
- pool_out_weight: bfloat16 [2048, 2048], P('tp', 'sp'), may hold values from -0.09375 to 0.09375
Outputs:
- mixed_rows: bfloat16 [1280, 2048], P(('grp', 'sp', 'tp')), parts along dimension 0
- log_totals: float32 [2, 16, 1280], P(None, 'tp', ('grp', 'sp')), parts along dimension 2
There are 2 independent parts, one for each index of `grp`. A program takes and returns all parts, laid end to end along the dimension named above; an argument that names none is the same for every part. Nothing has to cross between parts.
All inputs are finite; a program needn't handle non-finite values.
Results may differ from a plain program's by a relative error of at most 0.013.
The roundings to bfloat16 on the way count: a program that leaves them out, or rounds other values in their place, can miss the bound.
Values may be sent and summed in bfloat16 or wider, within the bound.
A program may use at most 64 MiB of HBM per device.

v0:
```python
import functools
import math

import jax
import jax.numpy as jnp
from jax import lax
from jax.experimental import pallas as pl
from jax.experimental.pallas import tpu as pltpu
from jax.sharding import PartitionSpec as P

HD = 64
VD = 128
POOL_SPAN = 16


epsilon = 1e-06
very_low = -1e30


def extended(cells, sides, width):
    for axis, dim in sides:
        count = lax.axis_size(axis)
        ends = count - 1
        head = lax.slice_in_dim(cells, 0, width, axis=dim)
        tail = lax.slice_in_dim(cells, cells.shape[dim] - width, cells.shape[dim], axis=dim)
        cells = jnp.concatenate(
            [
                lax.ppermute(tail, axis, [(i, (i + 1) % count) for i in range(ends)]),
                cells,
                lax.ppermute(head, axis, [((i + 1) % count, i) for i in range(ends)]),
            ],
            axis=dim,
        )
    return cells


def add_products(totals, pieces, source):
    results = []
    for running, piece in zip(totals, pieces):
        results.append(jnp.dot(source, piece, preferred_element_type=jnp.float32))
    return tuple(results)


def on_device(
    tokens,
    norm_gain,
    query_weight,
    key_weight,
    value_weight,
    map_lambda,
    head_gain,
    attn_out_weight,
    pool_out_weight,
):
    tokens_wide = tokens.astype(jnp.float32)
    normed = (
        tokens_wide
        * lax.rsqrt(jnp.mean(tokens_wide * tokens_wide, axis=-1, keepdims=True) + epsilon)
        * norm_gain
    ).astype(jnp.bfloat16)
    row_count = normed.shape[0]
    sp_index = lax.axis_index("sp")
    tp_index = lax.axis_index("tp")
    group_width = pool_out_weight.shape[0]
    local_heads = map_lambda.shape[0]
    key_heads = value_weight.shape[1] // VD
    group_heads = local_heads // key_heads
    q_empty = jnp.zeros((row_count, query_weight.shape[1]), jnp.float32)
    k_empty = jnp.zeros((row_count, key_weight.shape[1]), jnp.float32)
    v_empty = jnp.zeros((row_count, value_weight.shape[1]), jnp.float32)
    q_acc, k_acc, v_acc = add_products(
        (q_empty, k_empty, v_empty),
        (
            lax.all_gather(query_weight, "sp", axis=0, tiled=True),
            lax.all_gather(key_weight, "sp", axis=0, tiled=True),
            lax.all_gather(value_weight, "sp", axis=0, tiled=True),
        ),
        normed,
    )
    queries = q_acc.astype(jnp.bfloat16).reshape(row_count, key_heads, group_heads, 2, HD)
    keys_flat = k_acc.astype(jnp.bfloat16)
    values_flat = v_acc.astype(jnp.bfloat16)

    def key_block(state_now, key_pair):
        maxima, totals, accums = state_now
        key_blk, val_blk = key_pair
        scores = jnp.einsum(
            "qhgmd,khmd->hgmqk", queries, key_blk, preferred_element_type=jnp.float32
        ) * HD ** (-0.5)
        highest = jnp.maximum(maxima, jnp.max(scores, axis=-1))
        factor = jnp.exp(maxima - highest)
        weights = jnp.exp(scores - highest[..., None])
        totals = totals * factor + jnp.sum(weights, axis=-1)
        accums = accums * factor[..., None] + jnp.einsum(
            "hgmqk,khe->hgmqe",
            weights.astype(jnp.bfloat16),
            val_blk,
            preferred_element_type=jnp.float32,
        )
        return ((highest, totals, accums), None)

    start_state = (
        jnp.full((key_heads, group_heads, 2, row_count), very_low, jnp.float32),
        jnp.zeros((key_heads, group_heads, 2, row_count), jnp.float32),
        jnp.zeros((key_heads, group_heads, 2, row_count, VD), jnp.float32),
    )
    key_piece = lax.all_gather(keys_flat, "sp", axis=0, tiled=True)
    val_piece = lax.all_gather(values_flat, "sp", axis=0, tiled=True)
    piece_len = key_piece.shape[0]
    block_len = math.gcd(piece_len, 512)
    key_blocks = key_piece.reshape(piece_len // block_len, block_len, key_heads, 2, HD)
    val_blocks = val_piece.reshape(piece_len // block_len, block_len, key_heads, VD)
    state_next, unused = lax.scan(key_block, start_state, (key_blocks, val_blocks))
    maxima, totals, accums = state_next
    log_parts = maxima + jnp.log(totals)
    log_totals = jnp.transpose(log_parts, (2, 0, 1, 3)).reshape(2, local_heads, row_count)
    reads = accums / totals[..., None]
    contrast = reads[:, :, 0] - map_lambda.reshape(key_heads, group_heads, 1, 1) * reads[:, :, 1]
    scaled = (
        contrast
        * lax.rsqrt(jnp.mean(contrast * contrast, axis=-1, keepdims=True) + epsilon)
        * head_gain.reshape(key_heads, group_heads, 1, VD)
    )
    attention_head_rows = (
        jnp.transpose(scaled, (2, 0, 1, 3))
        .reshape(row_count, local_heads * VD)
        .astype(jnp.bfloat16)
    )
    head_rows, log_totals = (attention_head_rows, log_totals)
    own_chan = lax.dynamic_slice_in_dim(normed, tp_index * group_width, group_width, 1)
    reach = POOL_SPAN // 2
    padded = extended(own_chan, (("sp", 0),), reach)
    window = jnp.left_shift(jnp.int32(2), tp_index)
    half_span = window // 2
    running = jnp.zeros((row_count, group_width), jnp.float32)
    for offset in range(POOL_SPAN):
        piece = lax.dynamic_slice_in_dim(padded, reach - half_span + offset, row_count, 0).astype(
            jnp.float32
        )
        running = running + jnp.where(offset < window, piece, 0.0)
    seq_len = row_count * lax.axis_size("sp")
    position = sp_index * row_count + jnp.arange(row_count, dtype=jnp.int32)
    lower_edge = jnp.clip(position - half_span, 0, seq_len)
    upper_edge = jnp.clip(position + window - half_span, 0, seq_len)
    counts_f = (upper_edge - lower_edge).astype(jnp.float32)[:, None]
    pooled = (running / counts_f - own_chan.astype(jnp.float32)).astype(jnp.bfloat16)
    attn_whole, pool_whole = (
        lax.all_gather(attn_out_weight, "sp", axis=1, tiled=True),
        lax.all_gather(pool_out_weight, "sp", axis=1, tiled=True),
    )
    mixed = lax.psum_scatter(
        (
            jnp.dot(head_rows, attn_whole, preferred_element_type=jnp.float32)
            + jnp.dot(pooled, pool_whole, preferred_element_type=jnp.float32)
        ).astype(jnp.bfloat16),
        "tp",
        scatter_dimension=0,
        tiled=True,
    )
    return (mixed, log_totals)


MESH = pl.DeviceIdType.MESH
LANES = 128


def fused_kernel(
    count,
    tok,
    gain,
    wq,
    wk,
    wv,
    lam,
    hgain,
    wao,
    wpo,
    mixed_out,
    lt_out,
    tok_all,
    norm_all,
    w_all,
    q_all,
    k_all,
    v_all,
    heads_all,
    pooled_all,
    part_out,
    part_in,
    block_out,
    block_in,
    lt_send,
    lt_in,
    wao_in,
    wpo_in,
    local_sem,
    q_send,
    q_recv,
    z_send,
    z_recv,
    f_send,
    f_recv,
    h_send,
    h_recv,
    p_send,
    p_recv,
    o_send,
    o_recv,
    l_send,
    l_recv,
):
    g = lax.axis_index("grp")
    s = lax.axis_index("sp")
    t = lax.axis_index("tp")
    rows, width = tok.shape
    quarter = width // 4
    shard = wq.shape[0]
    half = shard // 2
    sib = t + 1 - 2 * lax.rem(t, 2)
    far = lax.rem(t + 2, 4)
    diag = lax.rem(sib + 2, 4)
    twin = 1 - g
    offs = list(range(1, count))
    order = sorted(offs, key=lambda o: min(o, count - o))
    f32, bf16 = jnp.float32, jnp.bfloat16

    def span(index, size):
        return pl.ds(pl.multiple_of(index * size, size), size)

    def half_rows(owner, part):
        return pl.ds(pl.multiple_of(owner * shard + part * half, half), half)

    pieces = (
        (tok, tok_all.at[span(s, rows), :]),
        (wk, w_all.at[span(s, shard), 0:LANES]),
        (wv, w_all.at[span(s, shard), LANES : 2 * LANES]),
        (wq.at[:, span(s, LANES)], w_all.at[span(s, shard), 2 * LANES : 3 * LANES]),
        (wao, wao_in),
        (wpo, wpo_in),
    )
    local = [
        pltpu.make_async_copy(src, dst, local_sem.at[i]) for i, (src, dst) in enumerate(pieces)
    ]
    for piece in local:
        piece.start()
    barrier = pltpu.get_barrier_semaphore()
    for off in offs:
        pl.semaphore_signal(
            barrier, inc=1, device_id={"sp": lax.rem(s + off, count)}, device_id_type=MESH
        )
    for peer in (sib, far, diag):
        pl.semaphore_signal(barrier, inc=1, device_id={"tp": peer}, device_id_type=MESH)
    pl.semaphore_signal(barrier, inc=1, device_id={"grp": twin}, device_id_type=MESH)
    pl.semaphore_wait(barrier, count - 1 + 4)

    def copy(src, dst, send, recv, where):
        return pltpu.make_async_remote_copy(
            src_ref=src,
            dst_ref=dst,
            send_sem=send,
            recv_sem=recv,
            device_id=where,
            device_id_type=MESH,
        )

    kv = slice(0, 2 * LANES)
    qs = slice(2 * LANES, 3 * LANES)

    def z_copy(kind, owner, up):
        if kind == 0:
            place = tok_all.at[span(owner, rows), span(t, quarter)]
        else:
            place = w_all.at[half_rows(owner, g), kv]
        step = 1 if up else -1
        return copy(
            place,
            place,
            z_send.at[kind, owner, int(up)],
            z_recv.at[kind, owner],
            {"sp": lax.rem(s + step + count, count)},
        )

    def q_copy(off):
        peer = lax.rem(s + off, count)
        src = wq.at[span(g, half), span(peer, LANES)]
        dst = w_all.at[half_rows(s, g), qs]
        return copy(src, dst, q_send.at[off], q_recv.at[s], {"sp": peer})

    def q_arrival(owner):
        place = w_all.at[half_rows(owner, g), qs]
        return copy(place, place, q_send.at[0], q_recv.at[owner], {"sp": owner})

    def tok_forward(step, owner):
        col = span(far if step == 2 else t, quarter)
        place = tok_all.at[span(owner, rows), col]
        where = {"tp": far if step == 1 else sib}
        return copy(place, place, f_send.at[step, owner], f_recv.at[step, owner], where)

    def w_forward(kind, owner):
        place = w_all.at[half_rows(owner, g), qs if kind else kv]
        at = 3 + kind
        return copy(place, place, f_send.at[at, owner], f_recv.at[at, owner], {"grp": twin})

    def sides(k, act):
        @pl.when(s >= k)
        def _():
            act(s - k, True, s < count - 1)

        @pl.when(s + k < count)
        def _():
            act(s + k, False, s > 0)

    def both_ways(act):
        @pl.when(s < count - 1)
        def _():
            act(True)

        @pl.when(s > 0)
        def _():
            act(False)

    local[0].wait()
    both_ways(lambda up: z_copy(0, s, up).start())
    local[1].wait()
    local[2].wait()
    both_ways(lambda up: z_copy(1, s, up).start())
    for off in order:
        q_copy(off).start()

    def norm_block(owner):
        step = 16

        def one(i, carry):
            at = pl.ds(pl.multiple_of(owner * rows + i * step, step), step)
            x = tok_all[at, :].astype(f32)
            scale = lax.rsqrt(jnp.mean(x * x, axis=-1, keepdims=True) + epsilon)
            norm_all[at, :] = (x * scale * gain[...]).astype(bf16)
            return carry

        lax.fori_loop(0, rows // step, one, 0)

    def z_tok(owner, up, more):
        z_copy(0, owner, True).wait_recv()

        @pl.when(more)
        def _():
            z_copy(0, owner, up).start()

        tok_forward(1, owner).start()
        tok_forward(0, owner).start()

    def z_weight(owner, up, more):
        z_copy(1, owner, True).wait_recv()

        @pl.when(more)
        def _():
            z_copy(1, owner, up).start()

        w_forward(0, owner).start()
        q_arrival(owner).wait_recv()
        w_forward(1, owner).start()

    def x_tok(owner, up, more):
        tok_forward(1, owner).wait_recv()
        tok_forward(2, owner).start()

    def norm_owner(owner, up, more):
        tok_forward(0, owner).wait_recv()
        tok_forward(2, owner).wait_recv()
        norm_block(owner)

    norm_block(s)
    last = count - 1
    for k in range(1, count):
        sides(k, z_tok)
        if k > 1:
            sides(k - 1, x_tok)
        if k > 2:
            sides(k - 2, norm_owner)
        sides(k, z_weight)
    if last > 1:
        sides(last - 1, norm_owner)
    sides(last, x_tok)
    sides(last, norm_owner)

    seq = rows * count
    group = wpo.shape[0]
    window = jnp.where(t == 0, 2, jnp.where(t == 1, 4, jnp.where(t == 2, 8, 16)))
    half_span = window // 2

    def pool(b, carry):
        at = b * rows + lax.broadcasted_iota(jnp.int32, (rows, seq), 0)
        col = lax.broadcasted_iota(jnp.int32, (rows, seq), 1)
        inside = (col >= at - half_span) & (col < at + window - half_span)
        band = jnp.where(inside, 1.0, 0.0).astype(bf16)
        total = jnp.dot(band, norm_all[:, span(t, group)], preferred_element_type=f32)
        pos = b * rows + lax.broadcasted_iota(jnp.int32, (rows, 1), 0)
        low = jnp.maximum(pos - half_span, 0)
        high = jnp.minimum(pos + window - half_span, seq)
        own = norm_all[span(b, rows), span(t, group)].astype(f32)
        pooled_all[span(b, rows), :] = (total / (high - low).astype(f32) - own).astype(bf16)
        return carry

    lax.fori_loop(0, count, pool, 0)

    def y_arrival(owner, up, more):
        w_forward(0, owner).wait_recv()
        w_forward(1, owner).wait_recv()

    for k in range(1, count):
        sides(k, y_arrival)
    local[3].wait()

    def project(b, carry):
        acc = jnp.dot(norm_all[span(b, rows), :], w_all[...], preferred_element_type=f32)
        k_all[span(b, rows), :] = acc[:, 0:LANES].astype(bf16)
        v_all[span(b, rows), :] = acc[:, LANES : 2 * LANES].astype(bf16)
        q_all[span(b, rows), :] = acc[:, 2 * LANES : 3 * LANES].astype(bf16)
        return carry

    lax.fori_loop(0, count, project, 0)

    def head_copy(b, off):
        place = heads_all.at[span(b, rows), span(s, LANES)]
        peer = lax.rem(s + off, count)
        return copy(place, place, h_send.at[b, off], h_recv.at[b, off], {"sp": peer})

    def lt_copy(b):
        return copy(lt_send.at[b], lt_in.at[s], l_send.at[b], l_recv.at[s], {"sp": b})

    lane = lax.broadcasted_iota(jnp.int32, (rows, LANES), 1)
    lt_rows = lt_send.shape[2]

    def attend(b, carry):
        q = q_all[span(b, rows), :]
        reads, logs = [], []
        for m in range(2):
            q_m = jnp.where((lane >= HD) == (m == 1), q, jnp.zeros_like(q))
            scores = (
                lax.dot_general(
                    q_m, k_all[...], (((1,), (1,)), ((), ())), preferred_element_type=f32
                )
                * HD ** (-0.5)
            )
            highest = jnp.max(scores, axis=-1, keepdims=True)
            weights = jnp.exp(scores - highest)
            totals = jnp.sum(weights, axis=-1, keepdims=True)
            reads.append(
                jnp.dot(weights.astype(bf16), v_all[...], preferred_element_type=f32) / totals
            )
            logs.append(highest + jnp.log(totals))
        contrast = reads[0] - lam[s] * reads[1]
        scaled = (
            contrast
            * lax.rsqrt(jnp.mean(contrast * contrast, axis=-1, keepdims=True) + epsilon)
            * hgain[pl.ds(s, 1), :]
        )
        heads_all[span(b, rows), span(s, LANES)] = scaled.astype(bf16)
        for off in order:
            head_copy(b, off).start()
        both = jnp.where(lane == 0, logs[0], logs[1])
        padded = jnp.concatenate([both, jnp.zeros((lt_rows - rows, LANES), f32)], axis=0)
        lt_send[b] = jnp.transpose(padded)[0:8, :]

        @pl.when(b != s)
        def _():
            lt_copy(b).start()

        return carry

    lax.fori_loop(0, count, attend, 0)

    sub = rows // 4
    peers = (sib, far, diag)

    def part_copy(b, j):
        return copy(
            part_out.at[b, peers[j]],
            part_in.at[b, j],
            p_send.at[b, j],
            p_recv.at[b, j],
            {"tp": peers[j]},
        )

    local[4].wait()
    local[5].wait()

    def out_copy(b):
        return copy(block_out.at[b], block_in.at[s], o_send.at[b], o_recv.at[s], {"sp": b})

    def finish(b):
        total = part_out[b, t].astype(f32)
        for j in range(3):
            part_copy(b, j).wait_recv()
            total = total + part_in[b, j].astype(f32)
        block_out[b] = total.astype(bf16)

        @pl.when(b != s)
        def _():
            out_copy(b).start()

    def outward(b, carry):
        for off in order:
            head_copy(b, off).wait_recv()
        total = jnp.dot(heads_all[span(b, rows), :], wao_in[...], preferred_element_type=f32)
        total = total + jnp.dot(
            pooled_all[span(b, rows), :], wpo_in[...], preferred_element_type=f32
        )
        for j in range(4):
            part_out[b, j] = total[j * sub : (j + 1) * sub, :].astype(bf16)
        for j in (2, 1, 0):
            part_copy(b, j).start()

        @pl.when(b > 0)
        def _():
            finish(b - 1)

        return carry

    lax.fori_loop(0, count, outward, 0)

    finish(count - 1)

    def put_logs(b, ref):
        for m in range(2):
            lt_out[m, b : b + 1, :] = ref[b, m : m + 1, 0:rows]

    for b in range(count):
        cols = slice(b * group, (b + 1) * group)

        @pl.when(s == b)
        def _():
            mixed_out[:, cols] = block_out[b]
            put_logs(b, lt_send)

        @pl.when(s != b)
        def _():
            copy(
                block_out.at[s], block_in.at[b], o_send.at[s], o_recv.at[b], {"sp": b}
            ).wait_recv()
            copy(lt_send.at[s], lt_in.at[b], l_send.at[s], l_recv.at[b], {"sp": b}).wait_recv()
            mixed_out[:, cols] = block_in[b]
            put_logs(b, lt_in)
            out_copy(b).wait_send()
            lt_copy(b).wait_send()

    both_ways(lambda up: z_copy(0, s, up).wait_send())
    both_ways(lambda up: z_copy(1, s, up).wait_send())
    for off in order:
        q_copy(off).wait_send()

    def sent(owner, up, more):
        @pl.when(more)
        def _():
            z_copy(0, owner, up).wait_send()
            z_copy(1, owner, up).wait_send()

        for step in range(3):
            tok_forward(step, owner).wait_send()
        w_forward(0, owner).wait_send()
        w_forward(1, owner).wait_send()

    for k in range(1, count):
        sides(k, sent)

    def drain(b, carry):
        for off in order:
            head_copy(b, off).wait_send()
        for j in range(3):
            part_copy(b, j).wait_send()
        return carry

    lax.fori_loop(0, count, drain, 0)


def fused(
    count,
    tokens,
    norm_gain,
    query_weight,
    key_weight,
    value_weight,
    map_lambda,
    head_gain,
    attn_out_weight,
    pool_out_weight,
):
    rows, width = tokens.shape
    cols = attn_out_weight.shape[1]
    sub = rows // 4
    seq = rows * count
    lt_rows = -(-rows // LANES) * LANES
    bf16, f32 = jnp.bfloat16, jnp.float32
    vmem = pl.BlockSpec(memory_space=pltpu.VMEM)
    smem = pl.BlockSpec(memory_space=pltpu.SMEM)
    far = pl.BlockSpec(memory_space=pl.ANY)
    sems = pltpu.SemaphoreType.DMA
    return pl.pallas_call(
        functools.partial(fused_kernel, count),
        out_shape=(
            jax.ShapeDtypeStruct((sub, width), bf16),
            jax.ShapeDtypeStruct((2, count, rows), f32),
        ),
        in_specs=[far, vmem, far, far, far, smem, vmem, far, far],
        out_specs=(vmem, vmem),
        scratch_shapes=[
            pltpu.VMEM((seq, width), bf16),
            pltpu.VMEM((seq, width), bf16),
            pltpu.VMEM((width, 3 * LANES), bf16),
            pltpu.VMEM((seq, LANES), bf16),
            pltpu.VMEM((seq, LANES), bf16),
            pltpu.VMEM((seq, LANES), bf16),
            pltpu.VMEM((seq, count * LANES), bf16),
            pltpu.VMEM((seq, pool_out_weight.shape[0]), bf16),
            pltpu.VMEM((count, 4, sub, cols), bf16),
            pltpu.VMEM((count, 3, sub, cols), bf16),
            pltpu.VMEM((count, sub, cols), bf16),
            pltpu.VMEM((count, sub, cols), bf16),
            pltpu.VMEM((count, 8, lt_rows), f32),
            pltpu.VMEM((count, 8, lt_rows), f32),
            pltpu.VMEM(attn_out_weight.shape, bf16),
            pltpu.VMEM(pool_out_weight.shape, bf16),
            sems((6,)),
            sems((count,)),
            sems((count,)),
            sems((2, count, 2)),
            sems((2, count)),
            sems((5, count)),
            sems((5, count)),
            sems((count, count)),
            sems((count, count)),
            sems((count, 3)),
            sems((count, 3)),
            sems((count,)),
            sems((count,)),
            sems((count,)),
            sems((count,)),
        ],
        compiler_params=pltpu.CompilerParams(collective_id=0, has_side_effects=True),
    )(
        tokens,
        norm_gain.reshape(1, width),
        query_weight,
        key_weight,
        value_weight,
        map_lambda,
        head_gain,
        attn_out_weight,
        pool_out_weight,
    )


def fits(shape, tokens, query_weight, value_weight, map_lambda, pool_out_weight):
    count = shape["sp"]
    return (
        shape["grp"] == 2
        and shape["tp"] == 4
        and count > 1
        and map_lambda.shape[0] == count
        and value_weight.shape[1] == VD == LANES == 2 * HD
        and tokens.shape[0] % 32 == 0
        and tokens.shape[1] % (4 * LANES) == 0
        and query_weight.shape[0] % 32 == 0
        and pool_out_weight.shape[0] * 4 == tokens.shape[1]
        and pool_out_weight.shape[1] % LANES == 0
        and pool_out_weight.shape[1] * count == tokens.shape[1]
        and pool_out_weight.shape[0] == pool_out_weight.shape[1]
        and tokens.shape[0] * count * tokens.shape[1] <= 1 << 22
    )


def solution(mesh):
    placed = (
        P(("grp", "sp"), None),
        P(),
        P("sp", "tp"),
        P("sp", "tp"),
        P("sp", "tp"),
        P("tp"),
        P("tp", None),
        P("tp", "sp"),
        P("tp", "sp"),
    )
    shape = dict(mesh.shape)

    def chosen(*args):
        if fits(shape, args[0], args[2], args[4], args[5], args[8]):
            return fused(shape["sp"], *args)
        return on_device(*args)

    return jax.shard_map(
        chosen,
        mesh=mesh,
        in_specs=placed,
        out_specs=(P(("grp", "sp", "tp"), None), P(None, "tp", ("grp", "sp"))),
        check_vma=False,
    )
```

profile of v0, /device:TPU:24, one launch (start us, length us, event | category | flops | bytes accessed | tf_op | source)
XLA Modules:
  0.0 62.9 jit_solution(9898441131046670579)
XLA Ops:
  0.6 60.0 %shard_map.104 = (bf16[40,2048]{1,0:T(8,128)(2,1)}, f32[2,4,160]{2,1,0:T(4,128)}) custom-call(bf16[160,2048]{1,0:T(8,128)(2,1)} %tok.1, f32[1,2048]{1,0:T(1,128)} %bitcast.1, bf16[512,512]{1,0:T(8,128)(2,1)} %wq.1, bf16[512,128]{1,0:T(8,128)(2,1)} %wk.1, bf16[512,128]{1,0:T(8,128)(2,1)} %wv.1, f32[4]{0:T(128)} %lam.1, f32[4,128]{1,0:T(4,128)} %hgain.1, ...), custom_call_target="tpu_custom_call" | custom-call | tf_op jit(solution)/shard_map/pallas_call | solution.py:598
  60.7 0.0 copy-start
  60.7 1.6 %copy.13 = bf16[40,2048]{1,0:T(8,128)(2,1)} copy(bf16[40,2048]{1,0:T(8,128)(2,1)} %get-tuple-element.4) | data formatting | bytes 327680
  62.3 0.0 copy-done
  62.3 0.6 copy.14
Async XLA Ops:
  60.7 1.6 %copy-start = (f32[2,4,160]{2,1,0:T(4,128)S(1)}, f32[2,4,160]{2,1,0:T(4,128)}, u32[]{:S(2)}) copy-start(f32[2,4,160]{2,1,0:T(4,128)} %get-tuple-element.5) | copy-start | bytes 15364
where the time goes:
time: 63.1 us; the launch traced here: 62.9 us
  Pallas kernels  60 us (95%)
  local copies, waits for them, and re-layouts  2.2 us (3%)
  between operations  0.65 us (1%)
    pallas_call x1, Pallas kernels, fused(): pl.pallas_call(functools.partial(fused_kernel, count), out_shape=(jax.Sha...  60 us
    unnamed x4, local copies, waits for them, and re-layouts  2.2 us

commit v1 on v0

--- a/solution.py
+++ b/solution.py
@@ -177,16 +177,25 @@
     wpo,
     mixed_out,
     lt_out,
-    tok_all,
+    tok_own,
     norm_all,
-    w_all,
+    kv_own,
+    q_own,
+    w_kv,
+    w_q,
+    par_own,
+    par_in,
+    par_use,
     q_all,
     k_all,
     v_all,
+    head_own,
     heads_all,
     pooled_all,
     part_out,
     part_in,
+    cross_out,
+    cross_in,
     block_out,
     block_in,
     lt_send,
@@ -194,16 +203,24 @@
     wao_in,
     wpo_in,
     local_sem,
-    q_send,
-    q_recv,
     z_send,
     z_recv,
     f_send,
     f_recv,
+    kv_send,
+    kv_recv,
+    q_send,
+    q_sib,
+    q_twin,
+    q_recv,
+    par_sem,
     h_send,
+    h_fwd,
     h_recv,
     p_send,
     p_recv,
+    x_send,
+    x_recv,
     o_send,
     o_recv,
     l_send,
@@ -212,46 +229,73 @@
     g = lax.axis_index("grp")
     s = lax.axis_index("sp")
     t = lax.axis_index("tp")
+    c = lax.rem(t, 2)
+    x = t // 2
     rows, width = tok.shape
     quarter = width // 4
     shard = wq.shape[0]
-    half = shard // 2
-    sib = t + 1 - 2 * lax.rem(t, 2)
+    part = shard // 2
+    half = s // 2
+    in_half = c == half
+    inner = (s > 0) & (s < count - 1)
+    sib = t + 1 - 2 * c
     far = lax.rem(t + 2, 4)
     diag = lax.rem(sib + 2, 4)
     twin = 1 - g
-    offs = list(range(1, count))
-    order = sorted(offs, key=lambda o: min(o, count - o))
+    outer = jnp.where(half == 1, count - 1, 0)
+    mate = 2 * half + 1 - lax.rem(s, 2)
+    beyond = jnp.where(half == 0, 2, 1)
+    near = jnp.where(c == 1, jnp.where(s == 2, 3, 2), jnp.where(s == 1, 0, 1))
+    home = 2 * x + half
+    mine = 2 * lax.rem(s, 2) + c
+    theirs = 2 * lax.rem(s, 2) + 1 - c
     f32, bf16 = jnp.float32, jnp.bfloat16
 
     def span(index, size):
         return pl.ds(pl.multiple_of(index * size, size), size)
 
-    def half_rows(owner, part):
-        return pl.ds(pl.multiple_of(owner * shard + part * half, half), half)
+    def half_rows(owner, which):
+        return pl.ds(pl.multiple_of(owner * shard + which * part, part), part)
 
     pieces = (
-        (tok, tok_all.at[span(s, rows), :]),
-        (wk, w_all.at[span(s, shard), 0:LANES]),
-        (wv, w_all.at[span(s, shard), LANES : 2 * LANES]),
-        (wq.at[:, span(s, LANES)], w_all.at[span(s, shard), 2 * LANES : 3 * LANES]),
+        (tok, tok_own),
+        (wk, kv_own.at[:, 0:LANES]),
+        (wv, kv_own.at[:, LANES : 2 * LANES]),
+        (wq, q_own),
         (wao, wao_in),
         (wpo, wpo_in),
     )
     local = [
         pltpu.make_async_copy(src, dst, local_sem.at[i]) for i, (src, dst) in enumerate(pieces)
     ]
+    own_pieces = (
+        (wk, w_kv.at[span(s, shard), 0:LANES]),
+        (wv, w_kv.at[span(s, shard), LANES : 2 * LANES]),
+        (wq.at[:, span(mine, LANES)], w_q.at[span(s, shard), :]),
+    )
+    own_local = [
+        pltpu.make_async_copy(src, dst, local_sem.at[len(pieces) + i])
+        for i, (src, dst) in enumerate(own_pieces)
+    ]
+    greeted = []
+    for off in range(1, count):
+        peer = lax.rem(s + off, count)
+        greeted += [{"sp": peer}, {"sp": peer, "tp": sib}]
+    greeted += [{"tp": sib}, {"tp": far}, {"grp": twin}, {"grp": twin, "tp": sib}]
+    barrier = pltpu.get_barrier_semaphore()
+    for where in greeted:
+        pl.semaphore_signal(barrier, inc=1, device_id=where, device_id_type=MESH)
     for piece in local:
         piece.start()
-    barrier = pltpu.get_barrier_semaphore()
-    for off in offs:
-        pl.semaphore_signal(
-            barrier, inc=1, device_id={"sp": lax.rem(s + off, count)}, device_id_type=MESH
-        )
-    for peer in (sib, far, diag):
-        pl.semaphore_signal(barrier, inc=1, device_id={"tp": peer}, device_id_type=MESH)
-    pl.semaphore_signal(barrier, inc=1, device_id={"grp": twin}, device_id_type=MESH)
-    pl.semaphore_wait(barrier, count - 1 + 4)
+
+    @pl.when(in_half)
+    def _():
+        for piece in own_local:
+            piece.start()
+
+    for i in range(count):
+        par_own[i : i + 1, :] = hgain[i : i + 1, :]
+        par_own[count + i : count + i + 1, :] = jnp.full((1, LANES), lam[i], f32)
 
     def copy(src, dst, send, recv, where):
         return pltpu.make_async_remote_copy(
@@ -263,43 +307,56 @@
             device_id_type=MESH,
         )
 
-    kv = slice(0, 2 * LANES)
-    qs = slice(2 * LANES, 3 * LANES)
-
-    def z_copy(kind, owner, up):
-        if kind == 0:
-            place = tok_all.at[span(owner, rows), span(t, quarter)]
-        else:
-            place = w_all.at[half_rows(owner, g), kv]
+    def z_copy(owner, up):
+        place = norm_all.at[span(owner, rows), span(t, quarter)]
         step = 1 if up else -1
-        return copy(
-            place,
-            place,
-            z_send.at[kind, owner, int(up)],
-            z_recv.at[kind, owner],
-            {"sp": lax.rem(s + step + count, count)},
-        )
-
-    def q_copy(off):
-        peer = lax.rem(s + off, count)
-        src = wq.at[span(g, half), span(peer, LANES)]
-        dst = w_all.at[half_rows(s, g), qs]
-        return copy(src, dst, q_send.at[off], q_recv.at[s], {"sp": peer})
-
-    def q_arrival(owner):
-        place = w_all.at[half_rows(owner, g), qs]
-        return copy(place, place, q_send.at[0], q_recv.at[owner], {"sp": owner})
+        where = {"sp": lax.rem(s + step + count, count)}
+        return copy(place, place, z_send.at[owner, int(up)], z_recv.at[owner], where)
 
     def tok_forward(step, owner):
         col = span(far if step == 2 else t, quarter)
-        place = tok_all.at[span(owner, rows), col]
+        place = norm_all.at[span(owner, rows), col]
         where = {"tp": far if step == 1 else sib}
         return copy(place, place, f_send.at[step, owner], f_recv.at[step, owner], where)
 
-    def w_forward(kind, owner):
-        place = w_all.at[half_rows(owner, g), qs if kind else kv]
-        at = 3 + kind
-        return copy(place, place, f_send.at[at, owner], f_recv.at[at, owner], {"grp": twin})
+    def kv_first():
+        src = kv_own.at[span(g, part), :]
+        return copy(src, w_kv.at[half_rows(s, g), :], kv_send.at[0, s], kv_recv.at[s, g], {"sp": near})
+
+    def kv_beside():
+        where = {"tp": sib}
+        return copy(kv_own, w_kv.at[span(s, shard), :], kv_send.at[1, s], kv_recv.at[s, 0], where)
+
+    spread = ({"sp": outer}, {"tp": sib}, {"grp": twin}, {"grp": twin, "tp": sib})
+
+    def kv_forward(kind, owner):
+        place = w_kv.at[half_rows(owner, g), :]
+        return copy(place, place, kv_send.at[kind, owner], kv_recv.at[owner, g], spread[kind])
+
+    def kv_arrival(owner, which):
+        place = w_kv.at[half_rows(owner, which), :]
+        return copy(place, place, kv_send.at[0, owner], kv_recv.at[owner, which], {"tp": sib})
+
+    def q_copy(r, core):
+        i = 2 * r + core
+        src = q_own.at[span(g, part), i * LANES : (i + 1) * LANES]
+        where = {"sp": 2 * c + r, "tp": 2 * x + core}
+        return copy(src, w_q.at[half_rows(s, g), :], q_send.at[r, core], q_recv.at[s, g], where)
+
+    def q_beside():
+        src = q_own.at[:, span(theirs, LANES)]
+        return copy(src, w_q.at[span(s, shard), :], q_sib.at[0], q_recv.at[s, 0], {"tp": sib})
+
+    def q_forward(owner):
+        place = w_q.at[half_rows(owner, g), :]
+        return copy(place, place, q_twin.at[owner], q_recv.at[owner, g], {"grp": twin})
+
+    def q_arrival(owner, which):
+        place = w_q.at[half_rows(owner, which), :]
+        return copy(place, place, q_twin.at[owner], q_recv.at[owner, which], {"grp": twin})
+
+    def par_copy():
+        return copy(par_own, par_in, par_sem.at[0], par_sem.at[1], {"tp": sib})
 
     def sides(k, act):
         @pl.when(s >= k)
@@ -319,69 +376,99 @@
         def _():
             act(False)
 
+    def each_q(act):
+        for r in range(2):
+
+            @pl.when(2 * c + r != s)
+            def _():
+                for core in range(2):
+                    act(r, core)
+
     local[0].wait()
-    both_ways(lambda up: z_copy(0, s, up).start())
+    step = rows // 2
+
+    def norm_rows(i, carry):
+        at = pl.ds(pl.multiple_of(i * step, step), step)
+        v = tok_own[at, :].astype(f32)
+        scale = lax.rsqrt(jnp.mean(v * v, axis=-1, keepdims=True) + epsilon)
+        to = pl.ds(pl.multiple_of(s * rows + i * step, step), step)
+        norm_all[to, :] = (v * scale * gain[...]).astype(bf16)
+        return carry
+
+    lax.fori_loop(0, rows // step, norm_rows, 0)
+    pl.semaphore_wait(barrier, len(greeted))
+    both_ways(lambda up: z_copy(s, up).start())
     local[1].wait()
     local[2].wait()
-    both_ways(lambda up: z_copy(1, s, up).start())
-    for off in order:
-        q_copy(off).start()
-
-    def norm_block(owner):
-        step = 16
-
-        def one(i, carry):
-            at = pl.ds(pl.multiple_of(owner * rows + i * step, step), step)
-            x = tok_all[at, :].astype(f32)
-            scale = lax.rsqrt(jnp.mean(x * x, axis=-1, keepdims=True) + epsilon)
-            norm_all[at, :] = (x * scale * gain[...]).astype(bf16)
-            return carry
-
-        lax.fori_loop(0, rows // step, one, 0)
+    kv_first().start()
+    local[3].wait()
+
+    @pl.when(in_half)
+    def _():
+        kv_beside().start()
+        q_beside().start()
+
+    par_copy().start()
+
+    @pl.when(jnp.logical_not(inner))
+    def _():
+        each_q(lambda r, core: q_copy(r, core).start())
 
     def z_tok(owner, up, more):
-        z_copy(0, owner, True).wait_recv()
+        z_copy(owner, True).wait_recv()
 
         @pl.when(more)
         def _():
-            z_copy(0, owner, up).start()
+            z_copy(owner, up).start()
 
         tok_forward(1, owner).start()
         tok_forward(0, owner).start()
-
-    def z_weight(owner, up, more):
-        z_copy(1, owner, True).wait_recv()
-
-        @pl.when(more)
-        def _():
-            z_copy(1, owner, up).start()
-
-        w_forward(0, owner).start()
-        q_arrival(owner).wait_recv()
-        w_forward(1, owner).start()
 
     def x_tok(owner, up, more):
         tok_forward(1, owner).wait_recv()
         tok_forward(2, owner).start()
 
-    def norm_owner(owner, up, more):
-        tok_forward(0, owner).wait_recv()
-        tok_forward(2, owner).wait_recv()
-        norm_block(owner)
-
-    norm_block(s)
+    def relays(owner):
+        return inner & (owner // 2 != half)
+
+    def z_kv(owner, up, more):
+        @pl.when(in_half)
+        def _():
+            kv_arrival(owner, g).wait_recv()
+
+            @pl.when(relays(owner))
+            def _():
+                kv_forward(0, owner).start()
+
+            for kind in (2, 3, 1):
+                kv_forward(kind, owner).start()
+
+    def z_q(owner, up, more):
+        q_arrival(owner, g).wait_recv()
+        q_forward(owner).start()
+
     last = count - 1
     for k in range(1, count):
         sides(k, z_tok)
         if k > 1:
             sides(k - 1, x_tok)
-        if k > 2:
-            sides(k - 2, norm_owner)
-        sides(k, z_weight)
-    if last > 1:
-        sides(last - 1, norm_owner)
+        sides(k, z_kv)
+        if k == 2:
+
+            @pl.when(inner)
+            def _():
+                each_q(lambda r, core: q_copy(r, core).start())
+
+    for k in range(1, count):
+        sides(k, z_q)
     sides(last, x_tok)
-    sides(last, norm_owner)
+
+    def tok_rest(owner, up, more):
+        tok_forward(0, owner).wait_recv()
+        tok_forward(2, owner).wait_recv()
+
+    for k in range(1, count):
+        sides(k, tok_rest)
 
     seq = rows * count
     group = wpo.shape[0]
@@ -403,127 +490,195 @@
 
     lax.fori_loop(0, count, pool, 0)
 
-    def y_arrival(owner, up, more):
-        w_forward(0, owner).wait_recv()
-        w_forward(1, owner).wait_recv()
+    def rest_kv(owner, up, more):
+        @pl.when(jnp.logical_not(in_half))
+        def _():
+            kv_arrival(owner, g).wait_recv()
+
+        kv_arrival(owner, twin).wait_recv()
 
     for k in range(1, count):
-        sides(k, y_arrival)
-    local[3].wait()
-
-    def project(b, carry):
-        acc = jnp.dot(norm_all[span(b, rows), :], w_all[...], preferred_element_type=f32)
+        sides(k, rest_kv)
+
+    @pl.when(in_half)
+    def _():
+        for piece in own_local:
+            piece.wait()
+
+    @pl.when(jnp.logical_not(in_half))
+    def _():
+        kv_beside().wait_recv()
+        q_beside().wait_recv()
+
+    def project_kv(b, carry):
+        acc = jnp.dot(norm_all[span(b, rows), :], w_kv[...], preferred_element_type=f32)
         k_all[span(b, rows), :] = acc[:, 0:LANES].astype(bf16)
         v_all[span(b, rows), :] = acc[:, LANES : 2 * LANES].astype(bf16)
-        q_all[span(b, rows), :] = acc[:, 2 * LANES : 3 * LANES].astype(bf16)
         return carry
 
-    lax.fori_loop(0, count, project, 0)
-
-    def head_copy(b, off):
-        place = heads_all.at[span(b, rows), span(s, LANES)]
-        peer = lax.rem(s + off, count)
-        return copy(place, place, h_send.at[b, off], h_recv.at[b, off], {"sp": peer})
+    lax.fori_loop(0, count, project_kv, 0)
+
+    def rest_q(owner, up, more):
+        q_arrival(owner, twin).wait_recv()
+
+    for k in range(1, count):
+        sides(k, rest_q)
+
+    def project_q(b, carry):
+        acc = jnp.dot(norm_all[span(b, rows), :], w_q[...], preferred_element_type=f32)
+        q_all[span(b, rows), :] = acc.astype(bf16)
+        return carry
+
+    lax.fori_loop(0, count, project_q, 0)
+
+    par_copy().wait_recv()
+    par_use[...] = jnp.where(in_half, par_own[...], par_in[...])
+
+    head_where = ({"sp": mate, "tp": home}, {"sp": beyond, "tp": home}, {"tp": sib})
+
+    def head_copy(kind, b):
+        src = head_own.at[span(b, rows), :]
+        dst = heads_all.at[span(b, rows), span(mine, LANES)]
+        return copy(src, dst, h_send.at[kind, b], h_recv.at[b, mine], head_where[kind])
+
+    def head_forward(b, i):
+        place = heads_all.at[span(b, rows), i * LANES : (i + 1) * LANES]
+        return copy(place, place, h_fwd.at[b, i], h_recv.at[b, i], {"sp": outer})
 
     def lt_copy(b):
-        return copy(lt_send.at[b], lt_in.at[s], l_send.at[b], l_recv.at[s], {"sp": b})
+        where = {"sp": b, "tp": home}
+        return copy(lt_send.at[b], lt_in.at[mine], l_send.at[b], l_recv.at[mine], where)
+
+    def lt_arrival(i):
+        return copy(lt_send.at[0], lt_in.at[i], l_send.at[0], l_recv.at[i], {"tp": sib})
 
     lane = lax.broadcasted_iota(jnp.int32, (rows, LANES), 1)
     lt_rows = lt_send.shape[2]
+    base = HD ** (-0.5)
 
     def attend(b, carry):
         q = q_all[span(b, rows), :]
-        reads, logs = [], []
-        for m in range(2):
-            q_m = jnp.where((lane >= HD) == (m == 1), q, jnp.zeros_like(q))
-            scores = (
-                lax.dot_general(
-                    q_m, k_all[...], (((1,), (1,)), ((), ())), preferred_element_type=f32
-                )
-                * HD ** (-0.5)
-            )
-            highest = jnp.max(scores, axis=-1, keepdims=True)
-            weights = jnp.exp(scores - highest)
-            totals = jnp.sum(weights, axis=-1, keepdims=True)
-            reads.append(
-                jnp.dot(weights.astype(bf16), v_all[...], preferred_element_type=f32) / totals
-            )
-            logs.append(highest + jnp.log(totals))
-        contrast = reads[0] - lam[s] * reads[1]
+        zero = jnp.zeros_like(q)
+        both_q = jnp.concatenate([jnp.where(lane < HD, q, zero), jnp.where(lane < HD, zero, q)], axis=0)
+        raw = lax.dot_general(
+            both_q, k_all[...], (((1,), (1,)), ((), ())), preferred_element_type=f32
+        )
+        highest = jnp.max(raw, axis=-1, keepdims=True)
+        weights = jnp.exp2((raw - highest) * (base * math.log2(math.e)))
+        totals = jnp.sum(weights, axis=-1, keepdims=True)
+        reads = jnp.dot(weights.astype(bf16), v_all[...], preferred_element_type=f32) / totals
+        logs = highest * base + jnp.log(totals)
+        contrast = reads[:rows] - par_use[pl.ds(count + mine, 1), :] * reads[rows:]
         scaled = (
             contrast
             * lax.rsqrt(jnp.mean(contrast * contrast, axis=-1, keepdims=True) + epsilon)
-            * hgain[pl.ds(s, 1), :]
-        )
-        heads_all[span(b, rows), span(s, LANES)] = scaled.astype(bf16)
-        for off in order:
-            head_copy(b, off).start()
-        both = jnp.where(lane == 0, logs[0], logs[1])
+            * par_use[pl.ds(mine, 1), :]
+        ).astype(bf16)
+        head_own[span(b, rows), :] = scaled
+
+        @pl.when(in_half)
+        def _():
+            heads_all[span(b, rows), span(mine, LANES)] = scaled
+
+        head_copy(1, b).start()
+        head_copy(0, b).start()
+
+        @pl.when(jnp.logical_not(in_half))
+        def _():
+            head_copy(2, b).start()
+
+        both = jnp.where(lane == 0, logs[:rows], logs[rows:])
         padded = jnp.concatenate([both, jnp.zeros((lt_rows - rows, LANES), f32)], axis=0)
         lt_send[b] = jnp.transpose(padded)[0:8, :]
 
-        @pl.when(b != s)
+        @pl.when(jnp.logical_not(in_half & (b == s)))
         def _():
             lt_copy(b).start()
 
         return carry
 
     lax.fori_loop(0, count, attend, 0)
-
-    sub = rows // 4
-    peers = (sib, far, diag)
-
-    def part_copy(b, j):
-        return copy(
-            part_out.at[b, peers[j]],
-            part_in.at[b, j],
-            p_send.at[b, j],
-            p_recv.at[b, j],
-            {"tp": peers[j]},
-        )
 
     local[4].wait()
     local[5].wait()
+    sub = rows // 4
+    is_relay = inner & jnp.logical_not(in_half)
+
+    def part_copy(b):
+        where = {"tp": sib}
+        return copy(part_out.at[b, 1 - c], part_in.at[b], p_send.at[b], p_recv.at[b], where)
+
+    def cross_copy(b):
+        return copy(cross_out.at[b], cross_in.at[b], x_send.at[b], x_recv.at[b], {"tp": far})
 
     def out_copy(b):
         return copy(block_out.at[b], block_in.at[s], o_send.at[b], o_recv.at[s], {"sp": b})
 
-    def finish(b):
-        total = part_out[b, t].astype(f32)
-        for j in range(3):
-            part_copy(b, j).wait_recv()
-            total = total + part_in[b, j].astype(f32)
-        block_out[b] = total.astype(bf16)
-
-        @pl.when(b != s)
-        def _():
-            out_copy(b).start()
-
-    def outward(b, carry):
-        for off in order:
-            head_copy(b, off).wait_recv()
+    def first_sum(b):
+        for i in range(count):
+
+            @pl.when(jnp.logical_not(in_half & (mine == i)))
+            def _():
+                head_forward(b, i).wait_recv()
+
+            @pl.when(is_relay)
+            def _():
+                head_forward(b, i).start()
+
         total = jnp.dot(heads_all[span(b, rows), :], wao_in[...], preferred_element_type=f32)
         total = total + jnp.dot(
             pooled_all[span(b, rows), :], wpo_in[...], preferred_element_type=f32
         )
         for j in range(4):
-            part_out[b, j] = total[j * sub : (j + 1) * sub, :].astype(bf16)
-        for j in (2, 1, 0):
-            part_copy(b, j).start()
+            part_out[b, j % 2, j // 2] = total[j * sub : (j + 1) * sub, :].astype(bf16)
+        part_copy(b).start()
+
+    def second_sum(b):
+        part_copy(b).wait_recv()
+        cross_out[b] = (
+            part_out[b, c, 1 - x].astype(f32) + part_in[b, 1 - x].astype(f32)
+        ).astype(bf16)
+        cross_copy(b).start()
+
+    def third_sum(b):
+        cross_copy(b).wait_recv()
+        block_out[b] = (
+            part_out[b, c, x].astype(f32)
+            + part_in[b, x].astype(f32)
+            + cross_in[b].astype(f32)
+        ).astype(bf16)
+
+        @pl.when(b != s)
+        def _():
+            out_copy(b).start()
+
+    def outward(b, carry):
+        first_sum(b)
+        second_sum(b)
 
         @pl.when(b > 0)
         def _():
-            finish(b - 1)
+            third_sum(b - 1)
 
         return carry
 
     lax.fori_loop(0, count, outward, 0)
-
-    finish(count - 1)
-
-    def put_logs(b, ref):
+    third_sum(count - 1)
+
+    def put_logs(i, ref, at):
         for m in range(2):
-            lt_out[m, b : b + 1, :] = ref[b, m : m + 1, 0:rows]
+            lt_out[m, i : i + 1, :] = ref[at, m : m + 1, 0:rows]
+
+    for i in range(count):
+
+        @pl.when(in_half & (mine == i))
+        def _():
+            put_logs(i, lt_send, s)
+
+        @pl.when(jnp.logical_not(in_half & (mine == i)))
+        def _():
+            lt_arrival(i).wait_recv()
+            put_logs(i, lt_in, i)
 
     for b in range(count):
         cols = slice(b * group, (b + 1) * group)
@@ -531,43 +686,65 @@
         @pl.when(s == b)
         def _():
             mixed_out[:, cols] = block_out[b]
-            put_logs(b, lt_send)
 
         @pl.when(s != b)
         def _():
-            copy(
-                block_out.at[s], block_in.at[b], o_send.at[s], o_recv.at[b], {"sp": b}
-            ).wait_recv()
-            copy(lt_send.at[s], lt_in.at[b], l_send.at[s], l_recv.at[b], {"sp": b}).wait_recv()
+            where = {"sp": b}
+            copy(block_out.at[s], block_in.at[b], o_send.at[s], o_recv.at[b], where).wait_recv()
             mixed_out[:, cols] = block_in[b]
-            put_logs(b, lt_in)
             out_copy(b).wait_send()
+
+        @pl.when(jnp.logical_not(in_half & (s == b)))
+        def _():
             lt_copy(b).wait_send()
 
-    both_ways(lambda up: z_copy(0, s, up).wait_send())
-    both_ways(lambda up: z_copy(1, s, up).wait_send())
-    for off in order:
-        q_copy(off).wait_send()
+    both_ways(lambda up: z_copy(s, up).wait_send())
+    kv_first().wait_send()
+    par_copy().wait_send()
+    each_q(lambda r, core: q_copy(r, core).wait_send())
+
+    @pl.when(in_half)
+    def _():
+        kv_beside().wait_send()
+        q_beside().wait_send()
 
     def sent(owner, up, more):
         @pl.when(more)
         def _():
-            z_copy(0, owner, up).wait_send()
-            z_copy(1, owner, up).wait_send()
+            z_copy(owner, up).wait_send()
 
         for step in range(3):
             tok_forward(step, owner).wait_send()
-        w_forward(0, owner).wait_send()
-        w_forward(1, owner).wait_send()
+
+        @pl.when(in_half)
+        def _():
+            @pl.when(relays(owner))
+            def _():
+                kv_forward(0, owner).wait_send()
+
+            for kind in (1, 2, 3):
+                kv_forward(kind, owner).wait_send()
+
+        q_forward(owner).wait_send()
 
     for k in range(1, count):
         sides(k, sent)
 
     def drain(b, carry):
-        for off in order:
-            head_copy(b, off).wait_send()
-        for j in range(3):
-            part_copy(b, j).wait_send()
+        head_copy(0, b).wait_send()
+        head_copy(1, b).wait_send()
+
+        @pl.when(jnp.logical_not(in_half))
+        def _():
+            head_copy(2, b).wait_send()
+
+        @pl.when(is_relay)
+        def _():
+            for i in range(count):
+                head_forward(b, i).wait_send()
+
+        part_copy(b).wait_send()
+        cross_copy(b).wait_send()
         return carry
 
     lax.fori_loop(0, count, drain, 0)
@@ -587,6 +764,7 @@
 ):
     rows, width = tokens.shape
     cols = attn_out_weight.shape[1]
+    shard = query_weight.shape[0]
     sub = rows // 4
     seq = rows * count
     lt_rows = -(-rows // LANES) * LANES
@@ -604,33 +782,50 @@
         in_specs=[far, vmem, far, far, far, smem, vmem, far, far],
         out_specs=(vmem, vmem),
         scratch_shapes=[
+            pltpu.VMEM((rows, width), bf16),
             pltpu.VMEM((seq, width), bf16),
-            pltpu.VMEM((seq, width), bf16),
-            pltpu.VMEM((width, 3 * LANES), bf16),
+            pltpu.VMEM((shard, 2 * LANES), bf16),
+            pltpu.VMEM((shard, count * LANES), bf16),
+            pltpu.VMEM((width, 2 * LANES), bf16),
+            pltpu.VMEM((width, LANES), bf16),
+            pltpu.VMEM((2 * count, LANES), f32),
+            pltpu.VMEM((2 * count, LANES), f32),
+            pltpu.VMEM((2 * count, LANES), f32),
+            pltpu.VMEM((seq, LANES), bf16),
             pltpu.VMEM((seq, LANES), bf16),
             pltpu.VMEM((seq, LANES), bf16),
             pltpu.VMEM((seq, LANES), bf16),
             pltpu.VMEM((seq, count * LANES), bf16),
             pltpu.VMEM((seq, pool_out_weight.shape[0]), bf16),
-            pltpu.VMEM((count, 4, sub, cols), bf16),
-            pltpu.VMEM((count, 3, sub, cols), bf16),
+            pltpu.VMEM((count, 2, 2, sub, cols), bf16),
+            pltpu.VMEM((count, 2, sub, cols), bf16),
+            pltpu.VMEM((count, sub, cols), bf16),
+            pltpu.VMEM((count, sub, cols), bf16),
             pltpu.VMEM((count, sub, cols), bf16),
             pltpu.VMEM((count, sub, cols), bf16),
             pltpu.VMEM((count, 8, lt_rows), f32),
             pltpu.VMEM((count, 8, lt_rows), f32),
             pltpu.VMEM(attn_out_weight.shape, bf16),
             pltpu.VMEM(pool_out_weight.shape, bf16),
-            sems((6,)),
-            sems((count,)),
-            sems((count,)),
-            sems((2, count, 2)),
-            sems((2, count)),
-            sems((5, count)),
-            sems((5, count)),
+            sems((9,)),
+            sems((count, 2)),
+            sems((count,)),
+            sems((3, count)),
+            sems((3, count)),
+            sems((4, count)),
+            sems((count, 2)),
+            sems((2, 2)),
+            sems((1,)),
+            sems((count,)),
+            sems((count, 2)),
+            sems((2,)),
+            sems((3, count)),
             sems((count, count)),
             sems((count, count)),
-            sems((count, 3)),
-            sems((count, 3)),
+            sems((count,)),
+            sems((count,)),
+            sems((count,)),
+            sems((count,)),
             sems((count,)),
             sems((count,)),
             sems((count,)),
@@ -655,12 +850,13 @@
     return (
         shape["grp"] == 2
         and shape["tp"] == 4
-        and count > 1
+        and count == 4
         and map_lambda.shape[0] == count
         and value_weight.shape[1] == VD == LANES == 2 * HD
         and tokens.shape[0] % 32 == 0
         and tokens.shape[1] % (4 * LANES) == 0
         and query_weight.shape[0] % 32 == 0
+        and query_weight.shape[1] == count * LANES
         and pool_out_weight.shape[0] * 4 == tokens.shape[1]
         and pool_out_weight.shape[1] % LANES == 0
         and pool_out_weight.shape[1] * count == tokens.shape[1]

time: 63.1 us -> 66.7 us (1.057); the launches traced: 62.9 us -> 65.6 us
  Pallas kernels: 60 us -> 62.8 us
    pallas_call x1, Pallas kernels: 60 us -> 62.8 us  [fused(): pl.pallas_call(functools.partial(fused_kernel, count), out_shape=(jax.Sha...]
where the time goes in v1:
time: 66.7 us; the launch traced here: 65.6 us
  Pallas kernels  62.8 us (94%)
  local copies, waits for them, and re-layouts  2.2 us (3%)
    pallas_call x1, Pallas kernels, fused(): pl.pallas_call(functools.partial(fused_kernel, count), out_shape=(jax.Sha...  62.8 us
    unnamed x4, local copies, waits for them, and re-layouts  2.2 us

profile of v1, /device:TPU:24, one launch (start us, length us, event | category | flops | bytes accessed | tf_op | source)
XLA Modules:
  0.0 65.6 jit_solution(5507031632781859286)
XLA Ops:
  0.6 62.8 %shard_map.104 = (bf16[40,2048]{1,0:T(8,128)(2,1)}, f32[2,4,160]{2,1,0:T(4,128)}) custom-call(bf16[160,2048]{1,0:T(8,128)(2,1)} %tok.1, f32[1,2048]{1,0:T(1,128)} %bitcast.1, bf16[512,512]{1,0:T(8,128)(2,1)} %wq.1, bf16[512,128]{1,0:T(8,128)(2,1)} %wk.1, bf16[512,128]{1,0:T(8,128)(2,1)} %wv.1, f32[4]{0:T(128)} %lam.1, f32[4,128]{1,0:T(4,128)} %hgain.1, ...), custom_call_target="tpu_custom_call" | custom-call | tf_op jit(solution)/shard_map/pallas_call | solution.py:776
  63.4 0.0 copy-start
  63.4 1.6 %copy.13 = bf16[40,2048]{1,0:T(8,128)(2,1)} copy(bf16[40,2048]{1,0:T(8,128)(2,1)} %get-tuple-element.4) | data formatting | bytes 327680
  65.0 0.0 copy-done
  65.0 0.6 copy.14
Async XLA Ops:
  63.4 1.6 %copy-start = (f32[2,4,160]{2,1,0:T(4,128)S(1)}, f32[2,4,160]{2,1,0:T(4,128)}, u32[]{:S(2)}) copy-start(f32[2,4,160]{2,1,0:T(4,128)} %get-tuple-element.5) | copy-start | bytes 15364

commit v2 on v1

v2 whole, which is shorter than its diff:
```python
import functools
import math

import jax
import jax.numpy as jnp
from jax import lax
from jax.experimental import pallas as pl
from jax.experimental.pallas import tpu as pltpu
from jax.sharding import PartitionSpec as P

HD = 64
VD = 128
POOL_SPAN = 16


epsilon = 1e-06
very_low = -1e30


def extended(cells, sides, width):
    for axis, dim in sides:
        count = lax.axis_size(axis)
        ends = count - 1
        head = lax.slice_in_dim(cells, 0, width, axis=dim)
        tail = lax.slice_in_dim(cells, cells.shape[dim] - width, cells.shape[dim], axis=dim)
        cells = jnp.concatenate(
            [
                lax.ppermute(tail, axis, [(i, (i + 1) % count) for i in range(ends)]),
                cells,
                lax.ppermute(head, axis, [((i + 1) % count, i) for i in range(ends)]),
            ],
            axis=dim,
        )
    return cells


def add_products(totals, pieces, source):
    results = []
    for running, piece in zip(totals, pieces):
        results.append(jnp.dot(source, piece, preferred_element_type=jnp.float32))
    return tuple(results)


def on_device(
    tokens,
    norm_gain,
    query_weight,
    key_weight,
    value_weight,
    map_lambda,
    head_gain,
    attn_out_weight,
    pool_out_weight,
):
    tokens_wide = tokens.astype(jnp.float32)
    normed = (
        tokens_wide
        * lax.rsqrt(jnp.mean(tokens_wide * tokens_wide, axis=-1, keepdims=True) + epsilon)
        * norm_gain
    ).astype(jnp.bfloat16)
    row_count = normed.shape[0]
    sp_index = lax.axis_index("sp")
    tp_index = lax.axis_index("tp")
    group_width = pool_out_weight.shape[0]
    local_heads = map_lambda.shape[0]
    key_heads = value_weight.shape[1] // VD
    group_heads = local_heads // key_heads
    q_empty = jnp.zeros((row_count, query_weight.shape[1]), jnp.float32)
    k_empty = jnp.zeros((row_count, key_weight.shape[1]), jnp.float32)
    v_empty = jnp.zeros((row_count, value_weight.shape[1]), jnp.float32)
    q_acc, k_acc, v_acc = add_products(
        (q_empty, k_empty, v_empty),
        (
            lax.all_gather(query_weight, "sp", axis=0, tiled=True),
            lax.all_gather(key_weight, "sp", axis=0, tiled=True),
            lax.all_gather(value_weight, "sp", axis=0, tiled=True),
        ),
        normed,
    )
    queries = q_acc.astype(jnp.bfloat16).reshape(row_count, key_heads, group_heads, 2, HD)
    keys_flat = k_acc.astype(jnp.bfloat16)
    values_flat = v_acc.astype(jnp.bfloat16)

    def key_block(state_now, key_pair):
        maxima, totals, accums = state_now
        key_blk, val_blk = key_pair
        scores = jnp.einsum(
            "qhgmd,khmd->hgmqk", queries, key_blk, preferred_element_type=jnp.float32
        ) * HD ** (-0.5)
        highest = jnp.maximum(maxima, jnp.max(scores, axis=-1))
        factor = jnp.exp(maxima - highest)
        weights = jnp.exp(scores - highest[..., None])
        totals = totals * factor + jnp.sum(weights, axis=-1)
        accums = accums * factor[..., None] + jnp.einsum(
            "hgmqk,khe->hgmqe",
            weights.astype(jnp.bfloat16),
            val_blk,
            preferred_element_type=jnp.float32,
        )
        return ((highest, totals, accums), None)

    start_state = (
        jnp.full((key_heads, group_heads, 2, row_count), very_low, jnp.float32),
        jnp.zeros((key_heads, group_heads, 2, row_count), jnp.float32),
        jnp.zeros((key_heads, group_heads, 2, row_count, VD), jnp.float32),
    )
    key_piece = lax.all_gather(keys_flat, "sp", axis=0, tiled=True)
    val_piece = lax.all_gather(values_flat, "sp", axis=0, tiled=True)
    piece_len = key_piece.shape[0]
    block_len = math.gcd(piece_len, 512)
    key_blocks = key_piece.reshape(piece_len // block_len, block_len, key_heads, 2, HD)
    val_blocks = val_piece.reshape(piece_len // block_len, block_len, key_heads, VD)
    state_next, unused = lax.scan(key_block, start_state, (key_blocks, val_blocks))
    maxima, totals, accums = state_next
    log_parts = maxima + jnp.log(totals)
    log_totals = jnp.transpose(log_parts, (2, 0, 1, 3)).reshape(2, local_heads, row_count)
    reads = accums / totals[..., None]
    contrast = reads[:, :, 0] - map_lambda.reshape(key_heads, group_heads, 1, 1) * reads[:, :, 1]
    scaled = (
        contrast
        * lax.rsqrt(jnp.mean(contrast * contrast, axis=-1, keepdims=True) + epsilon)
        * head_gain.reshape(key_heads, group_heads, 1, VD)
    )
    attention_head_rows = (
        jnp.transpose(scaled, (2, 0, 1, 3))
        .reshape(row_count, local_heads * VD)
        .astype(jnp.bfloat16)
    )
    head_rows, log_totals = (attention_head_rows, log_totals)
    own_chan = lax.dynamic_slice_in_dim(normed, tp_index * group_width, group_width, 1)
    reach = POOL_SPAN // 2
    padded = extended(own_chan, (("sp", 0),), reach)
    window = jnp.left_shift(jnp.int32(2), tp_index)
    half_span = window // 2
    running = jnp.zeros((row_count, group_width), jnp.float32)
    for offset in range(POOL_SPAN):
        piece = lax.dynamic_slice_in_dim(padded, reach - half_span + offset, row_count, 0).astype(
            jnp.float32
        )
        running = running + jnp.where(offset < window, piece, 0.0)
    seq_len = row_count * lax.axis_size("sp")
    position = sp_index * row_count + jnp.arange(row_count, dtype=jnp.int32)
    lower_edge = jnp.clip(position - half_span, 0, seq_len)
    upper_edge = jnp.clip(position + window - half_span, 0, seq_len)
    counts_f = (upper_edge - lower_edge).astype(jnp.float32)[:, None]
    pooled = (running / counts_f - own_chan.astype(jnp.float32)).astype(jnp.bfloat16)
    attn_whole, pool_whole = (
        lax.all_gather(attn_out_weight, "sp", axis=1, tiled=True),
        lax.all_gather(pool_out_weight, "sp", axis=1, tiled=True),
    )
    mixed = lax.psum_scatter(
        (
            jnp.dot(head_rows, attn_whole, preferred_element_type=jnp.float32)
            + jnp.dot(pooled, pool_whole, preferred_element_type=jnp.float32)
        ).astype(jnp.bfloat16),
        "tp",
        scatter_dimension=0,
        tiled=True,
    )
    return (mixed, log_totals)


MESH = pl.DeviceIdType.MESH
LANES = 128
scope = jax.named_scope


def fused_kernel(
    count,
    tok,
    gain,
    wq,
    wk,
    wv,
    lam,
    hgain,
    wao,
    wpo,
    mixed_out,
    lt_out,
    tok_own,
    gain_own,
    lam_own,
    hgain_own,
    norm_all,
    kv_own,
    w_kv,
    w_q,
    wa_all,
    wp_all,
    par_own,
    par_in,
    par_use,
    q_all,
    k_all,
    v_all,
    head_own,
    heads_all,
    pooled_all,
    part_out,
    part_in,
    cross_out,
    cross_in,
    block_out,
    block_in,
    lt_send,
    lt_in,
    local_sem,
    z_send,
    z_recv,
    f_send,
    f_recv,
    kv_send,
    kv_fwd,
    kv_recv,
    q_send,
    q_twin,
    q_recv,
    w_send,
    w_fwd,
    w_recv,
    par_sem,
    h_send,
    h_recv,
    p_send,
    p_recv,
    x_send,
    x_recv,
    o_send,
    o_recv,
    l_send,
    l_recv,
):
    g = lax.axis_index("grp")
    s = lax.axis_index("sp")
    t = lax.axis_index("tp")
    c = lax.rem(t, 2)
    x = t // 2
    rows, width = tok.shape
    quarter = width // 4
    shard = wq.shape[0]
    part = shard // 2
    pair = 2 * LANES
    group = wpo.shape[0]
    cols = wpo.shape[1]
    half = s // 2
    inner = (s > 0) & (s < count - 1)
    at_home = inner & (c == half)
    away = inner & (c != half)
    sib = t + 1 - 2 * c
    far = lax.rem(t + 2, 4)
    twin = 1 - g
    near = 1 + half
    other = count - 1 - s
    edge = jnp.where(half == 0, 0, count - 1)
    far_edge = count - 1 - edge
    target = 1 + c
    home = 2 * x + half
    f32, bf16 = jnp.float32, jnp.bfloat16

    def span(index, size):
        return pl.ds(pl.multiple_of(index * size, size), size)

    def half_rows(owner, which):
        return pl.ds(pl.multiple_of(owner * shard + which * part, part), part)

    barrier = pltpu.get_barrier_semaphore()

    def greet(where):
        pl.semaphore_signal(barrier, inc=1, device_id=where, device_id_type=MESH)

    for off in range(1, count):
        peer = lax.rem(s + off, count)
        peer_inner = (peer > 0) & (peer < count - 1)

        @pl.when(inner | peer_inner)
        def _():
            greet({"sp": peer})
            greet({"sp": peer, "tp": sib})

    @pl.when(inner)
    def _():
        greet({"tp": sib})
        greet({"tp": far})
        greet({"grp": twin})

    pieces = (
        (tok, tok_own),
        (gain, gain_own),
        (wk, kv_own.at[:, 0:LANES]),
        (wv, kv_own.at[:, LANES:pair]),
        (lam, lam_own),
        (hgain, hgain_own),
        (wao, wa_all.at[:, span(lax.rem(s, 2), cols)]),
        (wpo, wp_all.at[:, span(lax.rem(s, 2), cols)]),
        (wk, w_kv.at[span(s, shard), 0:LANES]),
        (wv, w_kv.at[span(s, shard), LANES:pair]),
        (wq.at[:, span(c, pair)], w_q.at[span(s, shard), :]),
    )
    local = [
        pltpu.make_async_copy(src, dst, local_sem.at[i]) for i, (src, dst) in enumerate(pieces)
    ]
    for piece in local[:4]:
        piece.start()

    @pl.when(inner)
    def _():
        for piece in local[4:8]:
            piece.start()

    @pl.when(at_home)
    def _():
        for piece in local[8:]:
            piece.start()

    def copy(src, dst, send, recv, where):
        return pltpu.make_async_remote_copy(
            src_ref=src,
            dst_ref=dst,
            send_sem=send,
            recv_sem=recv,
            device_id=where,
            device_id_type=MESH,
        )

    def z_copy(owner, dest):
        place = norm_all.at[span(owner, rows), span(t, quarter)]
        return copy(place, place, z_send.at[owner], z_recv.at[owner], {"sp": dest})

    def tok_forward(step, owner):
        col = span(far if step == 2 else t, quarter)
        place = norm_all.at[span(owner, rows), col]
        where = {"tp": far if step == 1 else sib}
        return copy(place, place, f_send.at[step, owner], f_recv.at[step, owner], where)

    def kv_first():
        src = kv_own.at[span(g, part), :]
        dst = w_kv.at[half_rows(s, g), :]
        return copy(src, dst, kv_send.at[0], kv_recv.at[s, g], {"sp": target})

    def kv_beside():
        dst = w_kv.at[span(s, shard), :]
        return copy(kv_own, dst, kv_send.at[1], kv_recv.at[s, 0], {"tp": sib})

    def kv_forward(kind, owner):
        which = twin if kind == 2 else g
        place = w_kv.at[half_rows(owner, which), :]
        where = {"grp": twin} if kind == 0 else {"tp": sib}
        return copy(place, place, kv_fwd.at[kind, owner], kv_recv.at[owner, which], where)

    def kv_arrival(owner, which):
        place = w_kv.at[half_rows(owner, which), :]
        return copy(place, place, kv_fwd.at[0, owner], kv_recv.at[owner, which], {"tp": sib})

    def q_copy(core):
        src = wq.at[span(g, part), core * pair : (core + 1) * pair]
        dst = w_q.at[half_rows(s, g), :]
        where = {"sp": target, "tp": 2 * x + core}
        return copy(src, dst, q_send.at[core], q_recv.at[s, g], where)

    def q_beside():
        src = wq.at[:, span(1 - c, pair)]
        return copy(src, w_q.at[span(s, shard), :], q_send.at[2], q_recv.at[s, 0], {"tp": sib})

    def q_forward(owner):
        place = w_q.at[half_rows(owner, g), :]
        return copy(place, place, q_twin.at[owner], q_recv.at[owner, g], {"grp": twin})

    def q_arrival(owner, which):
        place = w_q.at[half_rows(owner, which), :]
        return copy(place, place, q_twin.at[owner], q_recv.at[owner, which], {"grp": twin})

    stores = (wa_all, wp_all)

    def w_copy(kind):
        src = (wao, wpo)[kind].at[span(g, part), :]
        dst = stores[kind].at[span(g, part), span(lax.rem(s, 2), cols)]
        return copy(src, dst, w_send.at[kind], w_recv.at[kind, g], {"sp": near})

    def w_forward(kind):
        place = stores[kind].at[span(g, part), span(lax.rem(edge, 2), cols)]
        return copy(place, place, w_fwd.at[kind], w_recv.at[kind, g], {"grp": twin})

    def w_arrival(kind, which):
        place = stores[kind].at[span(which, part), span(lax.rem(edge, 2), cols)]
        return copy(place, place, w_fwd.at[kind], w_recv.at[kind, which], {"grp": twin})

    def par_copy():
        return copy(par_own, par_in, par_sem.at[0], par_sem.at[1], {"tp": sib})

    head_where = ({"sp": other, "tp": home}, {"tp": sib})

    def head_copy(kind, b, h):
        src = head_own.at[span(b, rows), span(h, LANES)]
        dst = heads_all.at[span(b, rows), span(2 * c + h, LANES)]
        return copy(src, dst, h_send.at[kind, b, h], h_recv.at[b, 2 * c + h], head_where[kind])

    def head_arrival(b, i):
        place = heads_all.at[span(b, rows), i * LANES : (i + 1) * LANES]
        return copy(place, place, h_send.at[0, b, 0], h_recv.at[b, i], {"tp": sib})

    def lt_copy(b):
        where = {"sp": b, "tp": home}
        return copy(lt_send.at[b], lt_in.at[c], l_send.at[b], l_recv.at[c], where)

    def lt_arrival(core):
        return copy(lt_send.at[0], lt_in.at[core], l_send.at[0], l_recv.at[core], {"tp": sib})

    def part_copy(b, e):
        src = part_out.at[b, e, 1 - c]
        return copy(src, part_in.at[b, e], p_send.at[b, e], p_recv.at[b, e], {"tp": sib})

    def cross_copy(b, e):
        src = cross_out.at[b, e]
        return copy(src, cross_in.at[b, e], x_send.at[b, e], x_recv.at[b, e], {"tp": far})

    def out_copy(b, e):
        to = 2 * half + e
        return copy(block_out.at[b, e], block_in.at[to], o_send.at[b, e], o_recv.at[to], {"sp": b})

    def out_arrival(i):
        return copy(block_out.at[0, 0], block_in.at[i], o_send.at[0, 0], o_recv.at[i], {"sp": near})

    local[0].wait()
    local[1].wait()
    step = rows // 2

    def norm_rows(i, carry):
        at = pl.ds(pl.multiple_of(i * step, step), step)
        v = tok_own[at, :].astype(f32)
        scale = lax.rsqrt(jnp.mean(v * v, axis=-1, keepdims=True) + epsilon)
        to = pl.ds(pl.multiple_of(s * rows + i * step, step), step)
        norm_all[to, :] = (v * scale * gain_own[...]).astype(bf16)
        return carry

    with scope("norm"):
        lax.fori_loop(0, rows // step, norm_rows, 0)
    with scope("barrier"):
        pl.semaphore_wait(barrier, jnp.where(inner, 9, 4))
    sends_on = s != target

    @pl.when(inner)
    def _():
        z_copy(s, other).start()

    @pl.when(jnp.logical_not(inner))
    def _():
        z_copy(s, near).start()

    local[2].wait()
    local[3].wait()

    @pl.when(sends_on)
    def _():
        kv_first().start()

    def outer_work():
        for core in range(2):
            q_copy(core).start()
        for kind in range(2):
            w_copy(kind).start()

    pl.when(jnp.logical_not(inner))(outer_work)

    def inner_work():
        @pl.when(at_home)
        def _():
            kv_beside().start()
            q_beside().start()

        local[4].wait()
        local[5].wait()
        par_own[0:count, :] = hgain_own[...]
        for i in range(count):
            par_own[count + i : count + i + 1, :] = jnp.full((1, LANES), lam_own[i], f32)

        @pl.when(at_home)
        def _():
            par_copy().start()

        def tok_in(owner, onward):
            z_copy(owner, other).wait_recv()
            if onward:
                z_copy(owner, other).start()
            tok_forward(1, owner).start()
            tok_forward(0, owner).start()

        def tok_x(owner):
            tok_forward(1, owner).wait_recv()
            tok_forward(2, owner).start()

        def kv_in(owner):
            @pl.when(at_home)
            def _():
                kv_arrival(owner, g).wait_recv()
                kv_forward(0, owner).start()
                kv_forward(1, owner).start()

        def kv_y(owner):
            @pl.when(at_home)
            def _():
                kv_arrival(owner, twin).wait_recv()
                kv_forward(2, owner).start()

        def q_in(owner):
            q_arrival(owner, g).wait_recv()
            q_forward(owner).start()

        owners = (edge, other, far_edge)
        with scope("tok0"):
            tok_in(edge, True)

        @pl.when(away)
        def _():
            for core in range(2):
                q_copy(core).start()

        with scope("tok1"):
            tok_in(other, False)
        with scope("kv0"):
            kv_in(edge)
        with scope("kv1"):
            kv_in(other)
        with scope("q0"):
            q_in(edge)
        with scope("x0"):
            tok_x(edge)
        with scope("x1"):
            tok_x(other)
        with scope("tok2"):
            tok_in(far_edge, False)
        with scope("kv2"):
            kv_in(far_edge)
        with scope("q1"):
            q_in(other)
        with scope("q2"):
            q_in(far_edge)
        with scope("kvy"):
            for owner in owners:
                kv_y(owner)
        with scope("x2"):
            tok_x(far_edge)
        with scope("rest"):
            for owner in owners:
                tok_forward(0, owner).wait_recv()
                tok_forward(2, owner).wait_recv()

        seq = rows * count
        window = jnp.where(t == 0, 2, jnp.where(t == 1, 4, jnp.where(t == 2, 8, 16)))
        half_span = window // 2

        def pool(b, carry):
            at = b * rows + lax.broadcasted_iota(jnp.int32, (rows, seq), 0)
            col = lax.broadcasted_iota(jnp.int32, (rows, seq), 1)
            inside = (col >= at - half_span) & (col < at + window - half_span)
            band = jnp.where(inside, 1.0, 0.0).astype(bf16)
            total = jnp.dot(band, norm_all[:, span(t, group)], preferred_element_type=f32)
            pos = b * rows + lax.broadcasted_iota(jnp.int32, (rows, 1), 0)
            low = jnp.maximum(pos - half_span, 0)
            high = jnp.minimum(pos + window - half_span, seq)
            own = norm_all[span(b, rows), span(t, group)].astype(f32)
            pooled_all[span(b, rows), :] = (total / (high - low).astype(f32) - own).astype(bf16)
            return carry

        with scope("pool"):
            lax.fori_loop(0, count, pool, 0)

        with scope("kvrest"):

            @pl.when(at_home)
            def _():
                local[8].wait()
                local[9].wait()
                local[10].wait()

            @pl.when(away)
            def _():
                for owner in owners:
                    kv_arrival(owner, g).wait_recv()
                    kv_arrival(owner, twin).wait_recv()
                kv_beside().wait_recv()
                q_beside().wait_recv()
                par_copy().wait_recv()

        def project_kv(b, carry):
            acc = jnp.dot(norm_all[span(b, rows), :], w_kv[...], preferred_element_type=f32)
            k_all[span(b, rows), :] = acc[:, 0:LANES].astype(bf16)
            v_all[span(b, rows), :] = acc[:, LANES:pair].astype(bf16)
            return carry

        with scope("projkv"):
            lax.fori_loop(0, count, project_kv, 0)

        with scope("qrest"):
            for owner in owners:
                q_arrival(owner, twin).wait_recv()

        def project_q(b, carry):
            acc = jnp.dot(norm_all[span(b, rows), :], w_q[...], preferred_element_type=f32)
            q_all[span(b, rows), :] = acc.astype(bf16)
            return carry

        with scope("projq"):
            lax.fori_loop(0, count, project_q, 0)

        with scope("wao"):
            w_arrival(0, g).wait_recv()
            w_forward(0).start()

        par_use[...] = jnp.where(at_home, par_own[...], par_in[...])
        lane = lax.broadcasted_iota(jnp.int32, (rows, LANES), 1)
        lt_rows = lt_send.shape[3]
        base = HD ** (-0.5)

        def attend(n, carry):
            b = n // 2
            h = lax.rem(n, 2)
            head = 2 * c + h
            q = q_all[span(b, rows), span(h, LANES)]
            zero = jnp.zeros_like(q)
            both_q = jnp.concatenate(
                [jnp.where(lane < HD, q, zero), jnp.where(lane < HD, zero, q)], axis=0
            )
            raw = lax.dot_general(
                both_q, k_all[...], (((1,), (1,)), ((), ())), preferred_element_type=f32
            )
            highest = jnp.max(raw, axis=-1, keepdims=True)
            weights = jnp.exp2((raw - highest) * (base * math.log2(math.e)))
            totals = jnp.sum(weights, axis=-1, keepdims=True)
            reads = jnp.dot(weights.astype(bf16), v_all[...], preferred_element_type=f32) / totals
            logs = highest * base + jnp.log(totals)
            contrast = reads[:rows] - par_use[pl.ds(count + head, 1), :] * reads[rows:]
            scaled = (
                contrast
                * lax.rsqrt(jnp.mean(contrast * contrast, axis=-1, keepdims=True) + epsilon)
                * par_use[pl.ds(head, 1), :]
            ).astype(bf16)
            head_own[span(b, rows), span(h, LANES)] = scaled

            @pl.when(at_home)
            def _():
                heads_all[span(b, rows), span(head, LANES)] = scaled

            head_copy(0, b, h).start()

            @pl.when(away)
            def _():
                head_copy(1, b, h).start()

            both = jnp.where(lane == 0, logs[:rows], logs[rows:])
            padded = jnp.concatenate([both, jnp.zeros((lt_rows - rows, LANES), f32)], axis=0)
            lt_send[b, h] = jnp.transpose(padded)[0:8, :]

            @pl.when((h == 1) & jnp.logical_not(at_home & (b == s)))
            def _():
                lt_copy(b).start()

            @pl.when(n == 3)
            def _():
                w_arrival(1, g).wait_recv()
                w_forward(1).start()

            return carry

        with scope("attend"):
            lax.fori_loop(0, 2 * count, attend, 0)

        sub = rows // 4
        with scope("wrest"):
            local[6].wait()
            local[7].wait()
            w_arrival(0, twin).wait_recv()
            w_arrival(1, twin).wait_recv()

        def first_sum(b, e):
            @pl.when(e == 0)
            def _():
                for i in range(count):

                    @pl.when(jnp.logical_not(at_home & (i // 2 == c)))
                    def _():
                        head_arrival(b, i).wait_recv()

            at = span(e, cols)
            total = jnp.dot(heads_all[span(b, rows), :], wa_all[:, at], preferred_element_type=f32)
            total = total + jnp.dot(
                pooled_all[span(b, rows), :], wp_all[:, at], preferred_element_type=f32
            )
            for j in range(4):
                part_out[b, e, j % 2, j // 2] = total[j * sub : (j + 1) * sub, :].astype(bf16)
            part_copy(b, e).start()

        def second_sum(b, e):
            part_copy(b, e).wait_recv()
            cross_out[b, e] = (
                part_out[b, e, c, 1 - x].astype(f32) + part_in[b, e, 1 - x].astype(f32)
            ).astype(bf16)
            cross_copy(b, e).start()

        def third_sum(b, e):
            cross_copy(b, e).wait_recv()
            block_out[b, e] = (
                part_out[b, e, c, x].astype(f32)
                + part_in[b, e, x].astype(f32)
                + cross_in[b, e].astype(f32)
            ).astype(bf16)

            @pl.when(b != s)
            def _():
                out_copy(b, e).start()

        def outward(n, carry):
            with scope("S1"):
                first_sum(n // 2, lax.rem(n, 2))
            with scope("S2"):
                second_sum(n // 2, lax.rem(n, 2))

            @pl.when(n > 0)
            def _():
                with scope("S3"):
                    third_sum((n - 1) // 2, lax.rem(n - 1, 2))

            return carry

        lax.fori_loop(0, 2 * count, outward, 0)
        with scope("S3last"):
            third_sum(count - 1, 1)

    pl.when(inner)(inner_work)

    def put_logs(core, ref, at):
        for h in range(2):
            for m in range(2):
                i = 2 * core + h
                lt_out[m, i : i + 1, :] = ref[at, h, m : m + 1, 0:rows]

    for core in range(2):

        @pl.when(at_home & (c == core))
        def _():
            put_logs(core, lt_send, s)

        @pl.when(jnp.logical_not(at_home & (c == core)))
        def _():
            lt_arrival(core).wait_recv()
            put_logs(core, lt_in, core)

    for i in range(count):
        with scope(f"final{i}"):
            at = slice(i * cols, (i + 1) * cols)

            @pl.when(s == 1 + i // 2)
            def _():
                mixed_out[:, at] = block_out[s, i % 2]

            @pl.when(s != 1 + i // 2)
            def _():
                out_arrival(i).wait_recv()
                mixed_out[:, at] = block_in[i]

    @pl.when(sends_on)
    def _():
        kv_first().wait_send()
        for core in range(2):
            q_copy(core).wait_send()

    @pl.when(jnp.logical_not(inner))
    def _():
        z_copy(s, near).wait_send()
        for kind in range(2):
            w_copy(kind).wait_send()

    @pl.when(at_home)
    def _():
        kv_beside().wait_send()
        q_beside().wait_send()
        par_copy().wait_send()
        for owner in (edge, other, far_edge):
            for kind in range(3):
                kv_forward(kind, owner).wait_send()

    @pl.when(inner)
    def _():
        z_copy(s, other).wait_send()
        z_copy(edge, other).wait_send()
        for owner in (edge, other, far_edge):
            for step in range(3):
                tok_forward(step, owner).wait_send()
            q_forward(owner).wait_send()
        for kind in range(2):
            w_forward(kind).wait_send()

        def drain(b, carry):
            for h in range(2):
                head_copy(0, b, h).wait_send()

                @pl.when(away)
                def _():
                    head_copy(1, b, h).wait_send()

                part_copy(b, h).wait_send()
                cross_copy(b, h).wait_send()

                @pl.when(b != s)
                def _():
                    out_copy(b, h).wait_send()

            @pl.when(jnp.logical_not(at_home & (b == s)))
            def _():
                lt_copy(b).wait_send()

            return carry

        lax.fori_loop(0, count, drain, 0)


def fused(
    count,
    tokens,
    norm_gain,
    query_weight,
    key_weight,
    value_weight,
    map_lambda,
    head_gain,
    attn_out_weight,
    pool_out_weight,
):
    rows, width = tokens.shape
    group, cols = pool_out_weight.shape
    shard = query_weight.shape[0]
    sub = rows // 4
    seq = rows * count
    pair = 2 * LANES
    lt_rows = -(-rows // LANES) * LANES
    bf16, f32 = jnp.bfloat16, jnp.float32
    vmem = pl.BlockSpec(memory_space=pltpu.VMEM)
    far = pl.BlockSpec(memory_space=pl.ANY)
    sems = pltpu.SemaphoreType.DMA
    return pl.pallas_call(
        functools.partial(fused_kernel, count),
        out_shape=(
            jax.ShapeDtypeStruct((sub, width), bf16),
            jax.ShapeDtypeStruct((2, count, rows), f32),
        ),
        in_specs=[far] * 9,
        out_specs=(vmem, vmem),
        scratch_shapes=[
            pltpu.VMEM((rows, width), bf16),
            pltpu.VMEM((1, width), f32),
            pltpu.SMEM((count,), f32),
            pltpu.VMEM((count, LANES), f32),
            pltpu.VMEM((seq, width), bf16),
            pltpu.VMEM((shard, pair), bf16),
            pltpu.VMEM((width, pair), bf16),
            pltpu.VMEM((width, pair), bf16),
            pltpu.VMEM((group, 2 * cols), bf16),
            pltpu.VMEM((group, 2 * cols), bf16),
            pltpu.VMEM((2 * count, LANES), f32),
            pltpu.VMEM((2 * count, LANES), f32),
            pltpu.VMEM((2 * count, LANES), f32),
            pltpu.VMEM((seq, pair), bf16),
            pltpu.VMEM((seq, LANES), bf16),
            pltpu.VMEM((seq, LANES), bf16),
            pltpu.VMEM((seq, pair), bf16),
            pltpu.VMEM((seq, count * LANES), bf16),
            pltpu.VMEM((seq, group), bf16),
            pltpu.VMEM((count, 2, 2, 2, sub, cols), bf16),
            pltpu.VMEM((count, 2, 2, sub, cols), bf16),
            pltpu.VMEM((count, 2, sub, cols), bf16),
            pltpu.VMEM((count, 2, sub, cols), bf16),
            pltpu.VMEM((count, 2, sub, cols), bf16),
            pltpu.VMEM((count, sub, cols), bf16),
            pltpu.VMEM((count, 2, 8, lt_rows), f32),
            pltpu.VMEM((2, 2, 8, lt_rows), f32),
            sems((11,)),
            sems((count,)),
            sems((count,)),
            sems((3, count)),
            sems((3, count)),
            sems((2,)),
            sems((3, count)),
            sems((count, 2)),
            sems((3,)),
            sems((count,)),
            sems((count, 2)),
            sems((2,)),
            sems((2,)),
            sems((2, 2)),
            sems((2,)),
            sems((2, count, 2)),
            sems((count, count)),
            sems((count, 2)),
            sems((count, 2)),
            sems((count, 2)),
            sems((count, 2)),
            sems((count, 2)),
            sems((count,)),
            sems((count,)),
            sems((2,)),
        ],
        compiler_params=pltpu.CompilerParams(collective_id=0, has_side_effects=True),
    )(
        tokens,
        norm_gain.reshape(1, width),
        query_weight,
        key_weight,
        value_weight,
        map_lambda,
        head_gain,
        attn_out_weight,
        pool_out_weight,
    )


def fits(shape, tokens, query_weight, value_weight, map_lambda, pool_out_weight):
    count = shape["sp"]
    return (
        shape["grp"] == 2
        and shape["tp"] == 4
        and count == 4
        and map_lambda.shape[0] == count
        and value_weight.shape[1] == VD == LANES == 2 * HD
        and tokens.shape[0] % 32 == 0
        and tokens.shape[1] % (4 * LANES) == 0
        and query_weight.shape[0] % 32 == 0
        and query_weight.shape[1] == count * LANES
        and pool_out_weight.shape[0] * 4 == tokens.shape[1]
        and pool_out_weight.shape[1] % LANES == 0
        and pool_out_weight.shape[1] * count == tokens.shape[1]
        and pool_out_weight.shape[0] == pool_out_weight.shape[1]
        and pool_out_weight.shape[0] == query_weight.shape[0]
        and tokens.shape[0] * count * tokens.shape[1] <= 1 << 22
    )


def solution(mesh):
    placed = (
        P(("grp", "sp"), None),
        P(),
        P("sp", "tp"),
        P("sp", "tp"),
        P("sp", "tp"),
        P("tp"),
        P("tp", None),
        P("tp", "sp"),
        P("tp", "sp"),
    )
    shape = dict(mesh.shape)

    def chosen(*args):
        if fits(shape, args[0], args[2], args[4], args[5], args[8]):
            return fused(shape["sp"], *args)
        return on_device(*args)

    return jax.shard_map(
        chosen,
        mesh=mesh,
        in_specs=placed,
        out_specs=(P(("grp", "sp", "tp"), None), P(None, "tp", ("grp", "sp"))),
        check_vma=False,
    )
```

time: 66.7 us -> 69.2 us (1.037); the launches traced: 65.6 us -> 69.1 us
  Pallas kernels: 62.8 us -> 66.2 us
    pallas_call x1, Pallas kernels: 62.8 us -> 66.2 us  [fused(): pl.pallas_call(functools.partial(fused_kernel, count), out_shape=(jax.Sha...]
where the time goes in v2:
time: 69.2 us; the launch traced here: 69.1 us
  Pallas kernels  66.2 us (96%)
  local copies, waits for them, and re-layouts  2.2 us (3%)
    pallas_call x1, Pallas kernels, fused(): pl.pallas_call(functools.partial(fused_kernel, count), out_shape=(jax.Sha...  66.2 us
    unnamed x4, local copies, waits for them, and re-layouts  2.2 us

profile of v2, /device:TPU:24, one launch (start us, length us, event | category | flops | bytes accessed | tf_op | source)
XLA Modules:
  0.0 69.1 jit_solution(16148028009733180464)
XLA Ops:
  0.6 66.2 %shard_map.104 = (bf16[40,2048]{1,0:T(8,128)(2,1)}, f32[2,4,160]{2,1,0:T(4,128)}) custom-call(bf16[160,2048]{1,0:T(8,128)(2,1)} %tok.1, f32[1,2048]{1,0:T(1,128)} %bitcast.1, bf16[512,512]{1,0:T(8,128)(2,1)} %wq.1, bf16[512,128]{1,0:T(8,128)(2,1)} %wk.1, bf16[512,128]{1,0:T(8,128)(2,1)} %wv.1, f32[4]{0:T(128)} %lam.1, f32[4,128]{1,0:T(4,128)} %hgain.1, ...), custom_call_target="tpu_custom_call" | custom-call | tf_op jit(solution)/shard_map/pallas_call | solution.py:840
  66.9 0.0 copy-start
  66.9 1.6 %copy.13 = bf16[40,2048]{1,0:T(8,128)(2,1)} copy(bf16[40,2048]{1,0:T(8,128)(2,1)} %get-tuple-element.4) | data formatting | bytes 327680
  68.5 0.0 copy-done
  68.5 0.6 copy.14
Async XLA Ops:
  66.9 1.6 %copy-start = (f32[2,4,160]{2,1,0:T(4,128)S(1)}, f32[2,4,160]{2,1,0:T(4,128)}, u32[]{:S(2)}) copy-start(f32[2,4,160]{2,1,0:T(4,128)} %get-tuple-element.5) | copy-start | bytes 15364

commit v3 on v2

--- a/solution.py
+++ b/solution.py
@@ -187,7 +187,7 @@
     w_kv,
     w_q,
     wa_all,
-    wp_all,
+    wp_own,
     par_own,
     par_in,
     par_use,
@@ -203,10 +203,12 @@
     cross_in,
     block_out,
     block_in,
+    pool_in,
     lt_send,
     lt_in,
     local_sem,
     z_send,
+    z_out,
     z_recv,
     f_send,
     f_recv,
@@ -217,7 +219,6 @@
     q_twin,
     q_recv,
     w_send,
-    w_fwd,
     w_recv,
     par_sem,
     h_send,
@@ -278,10 +279,11 @@
             greet({"sp": peer})
             greet({"sp": peer, "tp": sib})
 
+    greet({"tp": sib})
+    greet({"tp": far})
+
     @pl.when(inner)
     def _():
-        greet({"tp": sib})
-        greet({"tp": far})
         greet({"grp": twin})
 
     pieces = (
@@ -291,8 +293,8 @@
         (wv, kv_own.at[:, LANES:pair]),
         (lam, lam_own),
         (hgain, hgain_own),
-        (wao, wa_all.at[:, span(lax.rem(s, 2), cols)]),
-        (wpo, wp_all.at[:, span(lax.rem(s, 2), cols)]),
+        (wao, wa_all.at[0]),
+        (wpo, wp_own),
         (wk, w_kv.at[span(s, shard), 0:LANES]),
         (wv, w_kv.at[span(s, shard), LANES:pair]),
         (wq.at[:, span(c, pair)], w_q.at[span(s, shard), :]),
@@ -303,9 +305,11 @@
     for piece in local[:4]:
         piece.start()
 
+    local[7].start()
+
     @pl.when(inner)
     def _():
-        for piece in local[4:8]:
+        for piece in local[4:7]:
             piece.start()
 
     @pl.when(at_home)
@@ -323,24 +327,38 @@
             device_id_type=MESH,
         )
 
-    def z_copy(owner, dest):
-        place = norm_all.at[span(owner, rows), span(t, quarter)]
-        return copy(place, place, z_send.at[owner], z_recv.at[owner], {"sp": dest})
-
-    def tok_forward(step, owner):
+    chunk = rows // 2
+
+    def z_copy(u, dest):
+        place = norm_all.at[span(u, chunk), span(t, quarter)]
+        return copy(place, place, z_send.at[u], z_recv.at[u], {"sp": dest})
+
+    def z_outward(u):
+        place = norm_all.at[span(u, chunk), span(t, quarter)]
+        return copy(place, place, z_out.at[u], z_recv.at[u], {"sp": edge})
+
+    def tok_forward(step, u):
         col = span(far if step == 2 else t, quarter)
-        place = norm_all.at[span(owner, rows), col]
+        place = norm_all.at[span(u, chunk), col]
         where = {"tp": far if step == 1 else sib}
-        return copy(place, place, f_send.at[step, owner], f_recv.at[step, owner], where)
+        return copy(place, place, f_send.at[step, u], f_recv.at[step, u], where)
 
     def kv_first():
         src = kv_own.at[span(g, part), :]
         dst = w_kv.at[half_rows(s, g), :]
         return copy(src, dst, kv_send.at[0], kv_recv.at[s, g], {"sp": target})
 
+    def kv_first_whole():
+        dst = w_kv.at[span(s, shard), :]
+        return copy(kv_own, dst, kv_send.at[0], kv_recv.at[s, 0], {"sp": near})
+
     def kv_beside():
         dst = w_kv.at[span(s, shard), :]
         return copy(kv_own, dst, kv_send.at[1], kv_recv.at[s, 0], {"tp": sib})
+
+    def kv_edge():
+        place = w_kv.at[span(edge, shard), :]
+        return copy(place, place, kv_fwd.at[1, edge], kv_recv.at[edge, 0], {"tp": sib})
 
     def kv_forward(kind, owner):
         which = twin if kind == 2 else g
@@ -358,6 +376,16 @@
         where = {"sp": target, "tp": 2 * x + core}
         return copy(src, dst, q_send.at[core], q_recv.at[s, g], where)
 
+    def q_whole(core):
+        src = wq.at[:, core * pair : (core + 1) * pair]
+        dst = w_q.at[span(s, shard), :]
+        where = {"sp": near, "tp": 2 * x + core}
+        return copy(src, dst, q_send.at[core], q_recv.at[s, 0], where)
+
+    def q_edge():
+        place = w_q.at[span(edge, shard), :]
+        return copy(place, place, q_twin.at[edge], q_recv.at[edge, 0], {"tp": sib})
+
     def q_beside():
         src = wq.at[:, span(1 - c, pair)]
         return copy(src, w_q.at[span(s, shard), :], q_send.at[2], q_recv.at[s, 0], {"tp": sib})
@@ -370,34 +398,22 @@
         place = w_q.at[half_rows(owner, which), :]
         return copy(place, place, q_twin.at[owner], q_recv.at[owner, which], {"grp": twin})
 
-    stores = (wa_all, wp_all)
-
-    def w_copy(kind):
-        src = (wao, wpo)[kind].at[span(g, part), :]
-        dst = stores[kind].at[span(g, part), span(lax.rem(s, 2), cols)]
-        return copy(src, dst, w_send.at[kind], w_recv.at[kind, g], {"sp": near})
-
-    def w_forward(kind):
-        place = stores[kind].at[span(g, part), span(lax.rem(edge, 2), cols)]
-        return copy(place, place, w_fwd.at[kind], w_recv.at[kind, g], {"grp": twin})
-
-    def w_arrival(kind, which):
-        place = stores[kind].at[span(which, part), span(lax.rem(edge, 2), cols)]
-        return copy(place, place, w_fwd.at[kind], w_recv.at[kind, which], {"grp": twin})
+    def w_copy():
+        return copy(wao, wa_all.at[1], w_send.at[0], w_recv.at[0], {"sp": near})
 
     def par_copy():
         return copy(par_own, par_in, par_sem.at[0], par_sem.at[1], {"tp": sib})
 
     head_where = ({"sp": other, "tp": home}, {"tp": sib})
 
-    def head_copy(kind, b, h):
-        src = head_own.at[span(b, rows), span(h, LANES)]
-        dst = heads_all.at[span(b, rows), span(2 * c + h, LANES)]
-        return copy(src, dst, h_send.at[kind, b, h], h_recv.at[b, 2 * c + h], head_where[kind])
-
-    def head_arrival(b, i):
-        place = heads_all.at[span(b, rows), i * LANES : (i + 1) * LANES]
-        return copy(place, place, h_send.at[0, b, 0], h_recv.at[b, i], {"tp": sib})
+    def head_copy(kind, b):
+        dst = heads_all.at[span(b, rows), span(c, pair)]
+        src = head_own.at[span(b, rows), :]
+        return copy(src, dst, h_send.at[kind, b], h_recv.at[b, c], head_where[kind])
+
+    def head_arrival(b, core):
+        place = heads_all.at[span(b, rows), core * pair : (core + 1) * pair]
+        return copy(place, place, h_send.at[0, b], h_recv.at[b, core], {"tp": sib})
 
     def lt_copy(b):
         where = {"sp": b, "tp": home}
@@ -415,11 +431,20 @@
         return copy(src, cross_in.at[b, e], x_send.at[b, e], x_recv.at[b, e], {"tp": far})
 
     def out_copy(b, e):
-        to = 2 * half + e
+        to = s if e == 0 else edge
         return copy(block_out.at[b, e], block_in.at[to], o_send.at[b, e], o_recv.at[to], {"sp": b})
 
     def out_arrival(i):
         return copy(block_out.at[0, 0], block_in.at[i], o_send.at[0, 0], o_recv.at[i], {"sp": near})
+
+    def pool_copy(b):
+        dst = pool_in.at[half]
+        where = {"sp": b}
+        return copy(block_out.at[b, 0], dst, o_send.at[b, 0], o_recv.at[count + half], where)
+
+    def pool_arrival(i):
+        dst = pool_in.at[i]
+        return copy(block_out.at[0, 0], dst, o_send.at[0, 0], o_recv.at[count + i], {"sp": near})
 
     local[0].wait()
     local[1].wait()
@@ -436,29 +461,111 @@
     with scope("norm"):
         lax.fori_loop(0, rows // step, norm_rows, 0)
     with scope("barrier"):
-        pl.semaphore_wait(barrier, jnp.where(inner, 9, 4))
+        pl.semaphore_wait(barrier, jnp.where(inner, 9, 6))
     sends_on = s != target
 
     @pl.when(inner)
     def _():
-        z_copy(s, other).start()
+        z_copy(2 * s, other).start()
+        z_copy(2 * s + 1, other).start()
+        z_outward(2 * s).start()
+        z_outward(2 * s + 1).start()
 
     @pl.when(jnp.logical_not(inner))
     def _():
-        z_copy(s, near).start()
+        z_copy(2 * s, near).start()
+        z_copy(2 * s + 1, near).start()
 
     local[2].wait()
     local[3].wait()
 
-    @pl.when(sends_on)
+    sends_near = jnp.logical_not(inner) & (c == half)
+    sends_past = sends_on & jnp.logical_not(sends_near)
+
+    @pl.when(sends_near)
+    def _():
+        kv_first_whole().start()
+        for core in range(2):
+            q_whole(core).start()
+
+    @pl.when(sends_past)
     def _():
         kv_first().start()
-
-    def outer_work():
         for core in range(2):
             q_copy(core).start()
-        for kind in range(2):
-            w_copy(kind).start()
+
+    seq = rows * count
+    window = jnp.where(t == 0, 2, jnp.where(t == 1, 4, jnp.where(t == 2, 8, 16)))
+    half_span = window // 2
+    sub = rows // 4
+
+    def pool(b, carry):
+        at = b * rows + lax.broadcasted_iota(jnp.int32, (rows, seq), 0)
+        col = lax.broadcasted_iota(jnp.int32, (rows, seq), 1)
+        inside = (col >= at - half_span) & (col < at + window - half_span)
+        band = jnp.where(inside, 1.0, 0.0).astype(bf16)
+        total = jnp.dot(band, norm_all[:, span(t, group)], preferred_element_type=f32)
+        pos = b * rows + lax.broadcasted_iota(jnp.int32, (rows, 1), 0)
+        low = jnp.maximum(pos - half_span, 0)
+        high = jnp.minimum(pos + window - half_span, seq)
+        own = norm_all[span(b, rows), span(t, group)].astype(f32)
+        pooled_all[span(b, rows), :] = (total / (high - low).astype(f32) - own).astype(bf16)
+        return carry
+
+    def hand_parts(b, e, total):
+        for j in range(4):
+            part_out[b, e, j % 2, j // 2] = total[j * sub : (j + 1) * sub, :].astype(bf16)
+        part_copy(b, e).start()
+
+    def pool_product(b):
+        return jnp.dot(pooled_all[span(b, rows), :], wp_own[...], preferred_element_type=f32)
+
+    def second_sum(b, e):
+        part_copy(b, e).wait_recv()
+        cross_out[b, e] = (
+            part_out[b, e, c, 1 - x].astype(f32) + part_in[b, e, 1 - x].astype(f32)
+        ).astype(bf16)
+        cross_copy(b, e).start()
+
+    def third_sum(b, e, send):
+        cross_copy(b, e).wait_recv()
+        block_out[b, e] = (
+            part_out[b, e, c, x].astype(f32)
+            + part_in[b, e, x].astype(f32)
+            + cross_in[b, e].astype(f32)
+        ).astype(bf16)
+
+        @pl.when(b != s)
+        def _():
+            send().start()
+
+    def outer_work():
+        w_copy().start()
+        with scope("otok"):
+            for owner in (near, count - 1 - near, far_edge):
+                z_copy(2 * owner, near).wait_recv()
+                z_copy(2 * owner + 1, near).wait_recv()
+        with scope("opool"):
+            lax.fori_loop(0, count, pool, 0)
+        local[7].wait()
+
+        def outer_steps(m, carry):
+            @pl.when((m >= 1) & (m < count + 1))
+            def _():
+                second_sum(m - 1, 0)
+
+            @pl.when(m < count)
+            def _():
+                hand_parts(m, 0, pool_product(m))
+
+            @pl.when(m >= 2)
+            def _():
+                third_sum(m - 2, 0, lambda: pool_copy(m - 2))
+
+            return carry
+
+        with scope("osum"):
+            lax.fori_loop(0, count + 2, outer_steps, 0)
 
     pl.when(jnp.logical_not(inner))(outer_work)
 
@@ -478,16 +585,18 @@
         def _():
             par_copy().start()
 
-        def tok_in(owner, onward):
-            z_copy(owner, other).wait_recv()
+        def tok_in(u, onward):
+            z_copy(u, other).wait_recv()
             if onward:
-                z_copy(owner, other).start()
-            tok_forward(1, owner).start()
-            tok_forward(0, owner).start()
-
-        def tok_x(owner):
-            tok_forward(1, owner).wait_recv()
-            tok_forward(2, owner).start()
+                z_copy(u, other).start()
+            else:
+                z_outward(u).start()
+            tok_forward(1, u).start()
+            tok_forward(0, u).start()
+
+        def tok_x(u):
+            tok_forward(1, u).wait_recv()
+            tok_forward(2, u).start()
 
         def kv_in(owner):
             @pl.when(at_home)
@@ -507,63 +616,48 @@
             q_forward(owner).start()
 
         owners = (edge, other, far_edge)
+        split = (other, far_edge)
         with scope("tok0"):
-            tok_in(edge, True)
-
-        @pl.when(away)
-        def _():
-            for core in range(2):
-                q_copy(core).start()
-
+            tok_in(2 * edge, True)
+            tok_in(2 * other, False)
         with scope("tok1"):
-            tok_in(other, False)
-        with scope("kv0"):
-            kv_in(edge)
+            tok_in(2 * edge + 1, True)
+            tok_in(2 * other + 1, False)
         with scope("kv1"):
             kv_in(other)
-        with scope("q0"):
-            q_in(edge)
-        with scope("x0"):
-            tok_x(edge)
-        with scope("x1"):
-            tok_x(other)
+        with scope("kv0"):
+
+            @pl.when(at_home)
+            def _():
+                kv_edge().wait_recv()
+                kv_edge().start()
+
+        with scope("q1"):
+            q_in(other)
+        with scope("kvy1"):
+            kv_y(other)
         with scope("tok2"):
-            tok_in(far_edge, False)
+            tok_in(2 * far_edge, False)
+            tok_in(2 * far_edge + 1, False)
+        with scope("x01"):
+            for u in (2 * edge, 2 * other, 2 * edge + 1, 2 * other + 1):
+                tok_x(u)
         with scope("kv2"):
             kv_in(far_edge)
-        with scope("q1"):
-            q_in(other)
         with scope("q2"):
             q_in(far_edge)
-        with scope("kvy"):
-            for owner in owners:
-                kv_y(owner)
+        with scope("pool"):
+            lax.fori_loop(0, count, pool, 0)
         with scope("x2"):
-            tok_x(far_edge)
+            tok_x(2 * far_edge)
+            tok_x(2 * far_edge + 1)
+        with scope("kvy2"):
+            kv_y(far_edge)
         with scope("rest"):
             for owner in owners:
-                tok_forward(0, owner).wait_recv()
-                tok_forward(2, owner).wait_recv()
-
-        seq = rows * count
-        window = jnp.where(t == 0, 2, jnp.where(t == 1, 4, jnp.where(t == 2, 8, 16)))
-        half_span = window // 2
-
-        def pool(b, carry):
-            at = b * rows + lax.broadcasted_iota(jnp.int32, (rows, seq), 0)
-            col = lax.broadcasted_iota(jnp.int32, (rows, seq), 1)
-            inside = (col >= at - half_span) & (col < at + window - half_span)
-            band = jnp.where(inside, 1.0, 0.0).astype(bf16)
-            total = jnp.dot(band, norm_all[:, span(t, group)], preferred_element_type=f32)
-            pos = b * rows + lax.broadcasted_iota(jnp.int32, (rows, 1), 0)
-            low = jnp.maximum(pos - half_span, 0)
-            high = jnp.minimum(pos + window - half_span, seq)
-            own = norm_all[span(b, rows), span(t, group)].astype(f32)
-            pooled_all[span(b, rows), :] = (total / (high - low).astype(f32) - own).astype(bf16)
-            return carry
-
-        with scope("pool"):
-            lax.fori_loop(0, count, pool, 0)
+                for u in (2 * owner, 2 * owner + 1):
+                    tok_forward(0, u).wait_recv()
+                    tok_forward(2, u).wait_recv()
 
         with scope("kvrest"):
 
@@ -575,7 +669,8 @@
 
             @pl.when(away)
             def _():
-                for owner in owners:
+                kv_edge().wait_recv()
+                for owner in split:
                     kv_arrival(owner, g).wait_recv()
                     kv_arrival(owner, twin).wait_recv()
                 kv_beside().wait_recv()
@@ -592,7 +687,8 @@
             lax.fori_loop(0, count, project_kv, 0)
 
         with scope("qrest"):
-            for owner in owners:
+            q_edge().wait_recv()
+            for owner in split:
                 q_arrival(owner, twin).wait_recv()
 
         def project_q(b, carry):
@@ -603,20 +699,14 @@
         with scope("projq"):
             lax.fori_loop(0, count, project_q, 0)
 
-        with scope("wao"):
-            w_arrival(0, g).wait_recv()
-            w_forward(0).start()
-
         par_use[...] = jnp.where(at_home, par_own[...], par_in[...])
         lane = lax.broadcasted_iota(jnp.int32, (rows, LANES), 1)
-        lt_rows = lt_send.shape[3]
+        lt_rows = lt_send.shape[2]
         base = HD ** (-0.5)
 
-        def attend(n, carry):
-            b = n // 2
-            h = lax.rem(n, 2)
+        def one_head(b, h):
             head = 2 * c + h
-            q = q_all[span(b, rows), span(h, LANES)]
+            q = q_all[span(b, rows), h * LANES : (h + 1) * LANES]
             zero = jnp.zeros_like(q)
             both_q = jnp.concatenate(
                 [jnp.where(lane < HD, q, zero), jnp.where(lane < HD, zero, q)], axis=0
@@ -635,96 +725,84 @@
                 * lax.rsqrt(jnp.mean(contrast * contrast, axis=-1, keepdims=True) + epsilon)
                 * par_use[pl.ds(head, 1), :]
             ).astype(bf16)
-            head_own[span(b, rows), span(h, LANES)] = scaled
+            return scaled, logs[:rows], logs[rows:]
+
+        def attend(b):
+            done = [one_head(b, h) for h in range(2)]
+            for h in range(2):
+                head_own[span(b, rows), h * LANES : (h + 1) * LANES] = done[h][0]
+            head_copy(0, b).start()
+
+            @pl.when(away)
+            def _():
+                head_copy(1, b).start()
 
             @pl.when(at_home)
             def _():
-                heads_all[span(b, rows), span(head, LANES)] = scaled
-
-            head_copy(0, b, h).start()
-
-            @pl.when(away)
-            def _():
-                head_copy(1, b, h).start()
-
-            both = jnp.where(lane == 0, logs[:rows], logs[rows:])
+                heads_all[span(b, rows), span(c, pair)] = head_own[span(b, rows), :]
+
+            both = jnp.where(
+                lane < 2,
+                jnp.where(lane == 0, done[0][1], done[0][2]),
+                jnp.where(lane == 2, done[1][1], done[1][2]),
+            )
             padded = jnp.concatenate([both, jnp.zeros((lt_rows - rows, LANES), f32)], axis=0)
-            lt_send[b, h] = jnp.transpose(padded)[0:8, :]
-
-            @pl.when((h == 1) & jnp.logical_not(at_home & (b == s)))
+            lt_send[b] = jnp.transpose(padded)[0:8, :]
+
+            @pl.when(jnp.logical_not(at_home & (b == s)))
             def _():
                 lt_copy(b).start()
 
-            @pl.when(n == 3)
-            def _():
-                w_arrival(1, g).wait_recv()
-                w_forward(1).start()
+        def first_sum(b):
+            for core in range(2):
+
+                @pl.when(jnp.logical_not(at_home & (c == core)))
+                def _():
+                    head_arrival(b, core).wait_recv()
+
+            for e in range(2):
+                if e == 1:
+
+                    @pl.when(b == 0)
+                    def _():
+                        w_copy().wait_recv()
+
+                total = jnp.dot(
+                    heads_all[span(b, rows), :], wa_all[e], preferred_element_type=f32
+                )
+                hand_parts(b, e, total + pool_product(b) if e == 0 else total)
+
+        def steps(m, carry):
+            @pl.when(m < count)
+            def _():
+                with scope("att"):
+                    attend(m)
+
+            @pl.when(m == 2)
+            def _():
+                local[6].wait()
+                local[7].wait()
+
+            @pl.when((m >= 3) & (m < count + 3))
+            def _():
+                with scope("S2"):
+                    for e in range(2):
+                        second_sum(m - 3, e)
+
+            @pl.when((m >= 2) & (m < count + 2))
+            def _():
+                with scope("S1"):
+                    first_sum(m - 2)
+
+            @pl.when(m >= 4)
+            def _():
+                with scope("S3"):
+                    for e in range(2):
+                        third_sum(m - 4, e, lambda: out_copy(m - 4, e))
 
             return carry
 
-        with scope("attend"):
-            lax.fori_loop(0, 2 * count, attend, 0)
-
-        sub = rows // 4
-        with scope("wrest"):
-            local[6].wait()
-            local[7].wait()
-            w_arrival(0, twin).wait_recv()
-            w_arrival(1, twin).wait_recv()
-
-        def first_sum(b, e):
-            @pl.when(e == 0)
-            def _():
-                for i in range(count):
-
-                    @pl.when(jnp.logical_not(at_home & (i // 2 == c)))
-                    def _():
-                        head_arrival(b, i).wait_recv()
-
-            at = span(e, cols)
-            total = jnp.dot(heads_all[span(b, rows), :], wa_all[:, at], preferred_element_type=f32)
-            total = total + jnp.dot(
-                pooled_all[span(b, rows), :], wp_all[:, at], preferred_element_type=f32
-            )
-            for j in range(4):
-                part_out[b, e, j % 2, j // 2] = total[j * sub : (j + 1) * sub, :].astype(bf16)
-            part_copy(b, e).start()
-
-        def second_sum(b, e):
-            part_copy(b, e).wait_recv()
-            cross_out[b, e] = (
-                part_out[b, e, c, 1 - x].astype(f32) + part_in[b, e, 1 - x].astype(f32)
-            ).astype(bf16)
-            cross_copy(b, e).start()
-
-        def third_sum(b, e):
-            cross_copy(b, e).wait_recv()
-            block_out[b, e] = (
-                part_out[b, e, c, x].astype(f32)
-                + part_in[b, e, x].astype(f32)
-                + cross_in[b, e].astype(f32)
-            ).astype(bf16)
-
-            @pl.when(b != s)
-            def _():
-                out_copy(b, e).start()
-
-        def outward(n, carry):
-            with scope("S1"):
-                first_sum(n // 2, lax.rem(n, 2))
-            with scope("S2"):
-                second_sum(n // 2, lax.rem(n, 2))
-
-            @pl.when(n > 0)
-            def _():
-                with scope("S3"):
-                    third_sum((n - 1) // 2, lax.rem(n - 1, 2))
-
-            return carry
-
-        lax.fori_loop(0, 2 * count, outward, 0)
-        with scope("S3last"):
-            third_sum(count - 1, 1)
+        lax.fori_loop(0, 2 * count, steps, 0)
 
     pl.when(inner)(inner_work)
 
@@ -732,7 +810,7 @@
         for h in range(2):
             for m in range(2):
                 i = 2 * core + h
-                lt_out[m, i : i + 1, :] = ref[at, h, m : m + 1, 0:rows]
+                lt_out[m, i : i + 1, :] = ref[at, 2 * h + m : 2 * h + m + 1, 0:rows]
 
     for core in range(2):
 
@@ -748,17 +826,39 @@
     for i in range(count):
         with scope(f"final{i}"):
             at = slice(i * cols, (i + 1) * cols)
-
-            @pl.when(s == 1 + i // 2)
-            def _():
-                mixed_out[:, at] = block_out[s, i % 2]
-
-            @pl.when(s != 1 + i // 2)
+            maker = min(max(i, 1), count - 2)
+            e = 0 if i == maker else 1
+
+            @pl.when(s == maker)
+            def _():
+                mixed_out[:, at] = block_out[s, e]
+
+            @pl.when(s != maker)
             def _():
                 out_arrival(i).wait_recv()
                 mixed_out[:, at] = block_in[i]
 
-    @pl.when(sends_on)
+            if e == 1:
+                which = i // (count - 1)
+
+                @pl.when(s == i)
+                def _():
+                    both = mixed_out[:, at].astype(f32) + block_out[s, 0].astype(f32)
+                    mixed_out[:, at] = both.astype(bf16)
+
+                @pl.when(s != i)
+                def _():
+                    pool_arrival(which).wait_recv()
+                    both = mixed_out[:, at].astype(f32) + pool_in[which].astype(f32)
+                    mixed_out[:, at] = both.astype(bf16)
+
+    @pl.when(sends_near)
+    def _():
+        kv_first_whole().wait_send()
+        for core in range(2):
+            q_whole(core).wait_send()
+
+    @pl.when(sends_past)
     def _():
         kv_first().wait_send()
         for core in range(2):
@@ -766,38 +866,55 @@
 
     @pl.when(jnp.logical_not(inner))
     def _():
-        z_copy(s, near).wait_send()
-        for kind in range(2):
-            w_copy(kind).wait_send()
+        z_copy(2 * s, near).wait_send()
+        z_copy(2 * s + 1, near).wait_send()
+        w_copy().wait_send()
+
+        def drain_outer(b, carry):
+            part_copy(b, 0).wait_send()
+            cross_copy(b, 0).wait_send()
+
+            @pl.when(b != s)
+            def _():
+                pool_copy(b).wait_send()
+
+            return carry
+
+        lax.fori_loop(0, count, drain_outer, 0)
 
     @pl.when(at_home)
     def _():
         kv_beside().wait_send()
         q_beside().wait_send()
         par_copy().wait_send()
-        for owner in (edge, other, far_edge):
+        kv_edge().wait_send()
+        for owner in (other, far_edge):
             for kind in range(3):
                 kv_forward(kind, owner).wait_send()
 
     @pl.when(inner)
     def _():
-        z_copy(s, other).wait_send()
-        z_copy(edge, other).wait_send()
+        for owner in (s, edge):
+            z_copy(2 * owner, other).wait_send()
+            z_copy(2 * owner + 1, other).wait_send()
+        for owner in (s, other, far_edge):
+            z_outward(2 * owner).wait_send()
+            z_outward(2 * owner + 1).wait_send()
         for owner in (edge, other, far_edge):
             for step in range(3):
-                tok_forward(step, owner).wait_send()
+                tok_forward(step, 2 * owner).wait_send()
+                tok_forward(step, 2 * owner + 1).wait_send()
+        for owner in (other, far_edge):
             q_forward(owner).wait_send()
-        for kind in range(2):
-            w_forward(kind).wait_send()
 
         def drain(b, carry):
+            head_copy(0, b).wait_send()
+
+            @pl.when(away)
+            def _():
+                head_copy(1, b).wait_send()
+
             for h in range(2):
-                head_copy(0, b, h).wait_send()
-
-                @pl.when(away)
-                def _():
-                    head_copy(1, b, h).wait_send()
-
                 part_copy(b, h).wait_send()
                 cross_copy(b, h).wait_send()
 
@@ -840,8 +957,8 @@
     return pl.pallas_call(
         functools.partial(fused_kernel, count),
         out_shape=(
-            jax.ShapeDtypeStruct((sub, width), bf16),
-            jax.ShapeDtypeStruct((2, count, rows), f32),
+            pltpu.VMEM((sub, width), bf16),
+            pltpu.VMEM((2, count, rows), f32),
         ),
         in_specs=[far] * 9,
         out_specs=(vmem, vmem),
@@ -854,8 +971,8 @@
             pltpu.VMEM((shard, pair), bf16),
             pltpu.VMEM((width, pair), bf16),
             pltpu.VMEM((width, pair), bf16),
-            pltpu.VMEM((group, 2 * cols), bf16),
-            pltpu.VMEM((group, 2 * cols), bf16),
+            pltpu.VMEM((2, group, cols), bf16),
+            pltpu.VMEM((group, cols), bf16),
             pltpu.VMEM((2 * count, LANES), f32),
             pltpu.VMEM((2 * count, LANES), f32),
             pltpu.VMEM((2 * count, LANES), f32),
@@ -871,31 +988,32 @@
             pltpu.VMEM((count, 2, sub, cols), bf16),
             pltpu.VMEM((count, 2, sub, cols), bf16),
             pltpu.VMEM((count, sub, cols), bf16),
-            pltpu.VMEM((count, 2, 8, lt_rows), f32),
-            pltpu.VMEM((2, 2, 8, lt_rows), f32),
+            pltpu.VMEM((2, sub, cols), bf16),
+            pltpu.VMEM((count, 8, lt_rows), f32),
+            pltpu.VMEM((2, 8, lt_rows), f32),
             sems((11,)),
-            sems((count,)),
-            sems((count,)),
-            sems((3, count)),
-            sems((3, count)),
+            sems((2 * count,)),
+            sems((2 * count,)),
+            sems((2 * count,)),
+            sems((3, 2 * count)),
+            sems((3, 2 * count)),
             sems((2,)),
             sems((3, count)),
             sems((count, 2)),
             sems((3,)),
             sems((count,)),
             sems((count, 2)),
+            sems((1,)),
+            sems((1,)),
             sems((2,)),
-            sems((2,)),
-            sems((2, 2)),
-            sems((2,)),
-            sems((2, count, 2)),
-            sems((count, count)),
+            sems((2, count)),
             sems((count, 2)),
             sems((count, 2)),
             sems((count, 2)),
             sems((count, 2)),
             sems((count, 2)),
-            sems((count,)),
+            sems((count, 2)),
+            sems((count + 2,)),
             sems((count,)),
             sems((2,)),
         ],

time: 69.2 us -> 53.8 us (0.78)
  Pallas kernels: 66.2 us -> 51.7 us
  local copies, waits for them, and re-layouts: 2.2 us -> 1.27 us
    pallas_call x1, Pallas kernels: 66.2 us -> 51.7 us  [fused(): pl.pallas_call(functools.partial(fused_kernel, count), out_shape=(pltpu.V...]
    unnamed x4 -> x2, local copies, waits for them, and re-layouts: 2.2 us -> 1.27 us
where the time goes in v3:
time: 53.8 us; the launch traced here: 53.6 us
  Pallas kernels  51.7 us (96%)
  local copies, waits for them, and re-layouts  1.27 us (2%)
  between operations  0.64 us (1%)
    pallas_call x1, Pallas kernels, fused(): pl.pallas_call(functools.partial(fused_kernel, count), out_shape=(pltpu.V...  51.7 us
    unnamed x2, local copies, waits for them, and re-layouts  1.27 us

profile of v3, /device:TPU:24, one launch (start us, length us, event | category | flops | bytes accessed | tf_op | source)
XLA Modules:
  0.0 53.6 jit_solution(2348258838389546356)
XLA Ops:
  0.6 51.7 %shard_map.104 = (bf16[40,2048]{1,0:T(8,128)(2,1)S(1)}, f32[2,4,160]{2,1,0:T(4,128)S(1)}) custom-call(bf16[160,2048]{1,0:T(8,128)(2,1)} %tok.1, f32[1,2048]{1,0:T(1,128)} %bitcast.1, bf16[512,512]{1,0:T(8,128)(2,1)} %wq.1, bf16[512,128]{1,0:T(8,128)(2,1)} %wk.1, bf16[512,128]{1,0:T(8,128)(2,1)} %wv.1, f32[4]{0:T(128)} %lam.1, f32[4,128]{1,0:T(4,128)} %hgain.1, ...), custom_call_target="tpu_custom_call" | custom-call | tf_op jit(solution)/shard_map/pallas_call | solution.py:957
  52.4 0.7 %copy.13 = bf16[40,2048]{1,0:T(8,128)(2,1)} copy(bf16[40,2048]{1,0:T(8,128)(2,1)S(1)} %get-tuple-element.2) | data formatting | bytes 327680
  53.0 0.6 %copy.14 = f32[2,4,160]{2,1,0:T(4,128)} copy(f32[2,4,160]{2,1,0:T(4,128)S(1)} %get-tuple-element.3) | data formatting | bytes 10240

commit v4 on v3

--- a/solution.py
+++ b/solution.py
@@ -184,6 +184,9 @@
     hgain_own,
     norm_all,
     kv_own,
+    q_own,
+    kv_relay,
+    q_relay,
     w_kv,
     w_q,
     wa_all,
@@ -191,6 +194,8 @@
     par_own,
     par_in,
     par_use,
+    acc_kv,
+    acc_q,
     q_all,
     k_all,
     v_all,
@@ -208,7 +213,6 @@
     lt_in,
     local_sem,
     z_send,
-    z_out,
     z_recv,
     f_send,
     f_recv,
@@ -218,7 +222,9 @@
     q_send,
     q_twin,
     q_recv,
+    r_recv,
     w_send,
+    w_fwd,
     w_recv,
     par_sem,
     h_send,
@@ -298,12 +304,14 @@
         (wk, w_kv.at[span(s, shard), 0:LANES]),
         (wv, w_kv.at[span(s, shard), LANES:pair]),
         (wq.at[:, span(c, pair)], w_q.at[span(s, shard), :]),
+        (wq, q_own),
     )
     local = [
         pltpu.make_async_copy(src, dst, local_sem.at[i]) for i, (src, dst) in enumerate(pieces)
     ]
     for piece in local[:4]:
         piece.start()
+    local[11].start()
 
     local[7].start()
 
@@ -314,7 +322,7 @@
 
     @pl.when(at_home)
     def _():
-        for piece in local[8:]:
+        for piece in local[8:11]:
             piece.start()
 
     def copy(src, dst, send, recv, where):
@@ -331,17 +339,27 @@
 
     def z_copy(u, dest):
         place = norm_all.at[span(u, chunk), span(t, quarter)]
-        return copy(place, place, z_send.at[u], z_recv.at[u], {"sp": dest})
+        return copy(place, place, z_send.at[0], z_recv.at[u], {"sp": dest})
 
     def z_outward(u):
         place = norm_all.at[span(u, chunk), span(t, quarter)]
-        return copy(place, place, z_out.at[u], z_recv.at[u], {"sp": edge})
+        return copy(place, place, z_send.at[1], z_recv.at[u], {"sp": edge})
 
     def tok_forward(step, u):
         col = span(far if step == 2 else t, quarter)
         place = norm_all.at[span(u, chunk), col]
         where = {"tp": far if step == 1 else sib}
-        return copy(place, place, f_send.at[step, u], f_recv.at[step, u], where)
+        got = f_recv.at[u] if step == 1 else f_recv.at[2 * count + step // 2]
+        return copy(place, place, f_send.at[step], got, where)
+
+    def tok_late(step, u):
+        col = span(far if step == 2 else t, quarter)
+        place = norm_all.at[span(u, chunk), col]
+        got = f_recv.at[2 * count + 2 + step + lax.rem(u, 2)]
+        return copy(place, place, f_send.at[step], got, {"tp": sib})
+
+    def all_sent(ref, sem):
+        copy(ref, ref, sem, sem, {"tp": sib}).wait_send()
 
     def kv_first():
         src = kv_own.at[span(g, part), :]
@@ -358,48 +376,76 @@
 
     def kv_edge():
         place = w_kv.at[span(edge, shard), :]
-        return copy(place, place, kv_fwd.at[1, edge], kv_recv.at[edge, 0], {"tp": sib})
+        return copy(place, place, kv_fwd.at[0], kv_recv.at[edge, 0], {"tp": sib})
 
     def kv_forward(kind, owner):
         which = twin if kind == 2 else g
         place = w_kv.at[half_rows(owner, which), :]
         where = {"grp": twin} if kind == 0 else {"tp": sib}
-        return copy(place, place, kv_fwd.at[kind, owner], kv_recv.at[owner, which], where)
+        return copy(place, place, kv_fwd.at[0], kv_recv.at[owner, which], where)
 
     def kv_arrival(owner, which):
         place = w_kv.at[half_rows(owner, which), :]
-        return copy(place, place, kv_fwd.at[0, owner], kv_recv.at[owner, which], {"tp": sib})
+        return copy(place, place, kv_fwd.at[0], kv_recv.at[owner, which], {"tp": sib})
 
     def q_copy(core):
-        src = wq.at[span(g, part), core * pair : (core + 1) * pair]
+        src = q_own.at[span(g, part), core * pair : (core + 1) * pair]
         dst = w_q.at[half_rows(s, g), :]
         where = {"sp": target, "tp": 2 * x + core}
-        return copy(src, dst, q_send.at[core], q_recv.at[s, g], where)
+        return copy(src, dst, q_send.at[0], q_recv.at[s, g], where)
 
     def q_whole(core):
-        src = wq.at[:, core * pair : (core + 1) * pair]
+        src = q_own.at[:, core * pair : (core + 1) * pair]
         dst = w_q.at[span(s, shard), :]
         where = {"sp": near, "tp": 2 * x + core}
-        return copy(src, dst, q_send.at[core], q_recv.at[s, 0], where)
+        return copy(src, dst, q_send.at[0], q_recv.at[s, 0], where)
 
     def q_edge():
         place = w_q.at[span(edge, shard), :]
-        return copy(place, place, q_twin.at[edge], q_recv.at[edge, 0], {"tp": sib})
+        return copy(place, place, q_twin.at[0], q_recv.at[edge, 0], {"tp": sib})
+
+    def relay_copy(i):
+        if i == 0:
+            src, dst = kv_own.at[span(g, part), :], kv_relay
+        else:
+            src = q_own.at[span(g, part), (i - 1) * pair : i * pair]
+            dst = q_relay.at[i - 1]
+        send = kv_send.at[0] if i == 0 else q_send.at[0]
+        return copy(src, dst, send, r_recv.at[i], {"sp": near})
+
+    def relay_forward(i):
+        if i == 0:
+            dst = w_kv.at[half_rows(edge, g), :]
+            return copy(kv_relay, dst, kv_send.at[2], kv_recv.at[edge, g], {"sp": other})
+        dst = w_q.at[half_rows(edge, g), :]
+        where = {"sp": other, "tp": 2 * x + i - 1}
+        return copy(q_relay.at[i - 1], dst, q_send.at[2], q_recv.at[edge, g], where)
 
     def q_beside():
-        src = wq.at[:, span(1 - c, pair)]
-        return copy(src, w_q.at[span(s, shard), :], q_send.at[2], q_recv.at[s, 0], {"tp": sib})
+        src = q_own.at[:, span(1 - c, pair)]
+        return copy(src, w_q.at[span(s, shard), :], q_send.at[1], q_recv.at[s, 0], {"tp": sib})
 
     def q_forward(owner):
         place = w_q.at[half_rows(owner, g), :]
-        return copy(place, place, q_twin.at[owner], q_recv.at[owner, g], {"grp": twin})
+        return copy(place, place, q_twin.at[0], q_recv.at[owner, g], {"grp": twin})
 
     def q_arrival(owner, which):
         place = w_q.at[half_rows(owner, which), :]
-        return copy(place, place, q_twin.at[owner], q_recv.at[owner, which], {"grp": twin})
-
-    def w_copy():
-        return copy(wao, wa_all.at[1], w_send.at[0], w_recv.at[0], {"sp": near})
+        return copy(place, place, q_twin.at[0], q_recv.at[owner, which], {"grp": twin})
+
+    w_rows = (span(g, part // 2), pl.ds(part, part), span(twin, part // 2))
+
+    def w_copy(kind):
+        src, dst = wao.at[w_rows[kind], :], wa_all.at[1, w_rows[kind], :]
+        return copy(src, dst, w_send.at[kind], w_recv.at[kind], {"sp": near})
+
+    def w_forward():
+        place = wa_all.at[1, w_rows[0], :]
+        return copy(place, place, w_fwd.at[0], w_recv.at[2], {"grp": twin})
+
+    def w_arrival(kind):
+        place = wa_all.at[1, w_rows[kind], :]
+        return copy(place, place, w_fwd.at[0], w_recv.at[kind], {"grp": twin})
 
     def par_copy():
         return copy(par_own, par_in, par_sem.at[0], par_sem.at[1], {"tp": sib})
@@ -409,42 +455,42 @@
     def head_copy(kind, b):
         dst = heads_all.at[span(b, rows), span(c, pair)]
         src = head_own.at[span(b, rows), :]
-        return copy(src, dst, h_send.at[kind, b], h_recv.at[b, c], head_where[kind])
+        return copy(src, dst, h_send.at[kind], h_recv.at[b, c], head_where[kind])
 
     def head_arrival(b, core):
         place = heads_all.at[span(b, rows), core * pair : (core + 1) * pair]
-        return copy(place, place, h_send.at[0, b], h_recv.at[b, core], {"tp": sib})
+        return copy(place, place, h_send.at[0], h_recv.at[b, core], {"tp": sib})
 
     def lt_copy(b):
         where = {"sp": b, "tp": home}
-        return copy(lt_send.at[b], lt_in.at[c], l_send.at[b], l_recv.at[c], where)
+        return copy(lt_send.at[b], lt_in.at[c], l_send.at[0], l_recv.at[c], where)
 
     def lt_arrival(core):
         return copy(lt_send.at[0], lt_in.at[core], l_send.at[0], l_recv.at[core], {"tp": sib})
 
     def part_copy(b, e):
         src = part_out.at[b, e, 1 - c]
-        return copy(src, part_in.at[b, e], p_send.at[b, e], p_recv.at[b, e], {"tp": sib})
+        return copy(src, part_in.at[b, e], p_send.at[0], p_recv.at[b, e], {"tp": sib})
 
     def cross_copy(b, e):
         src = cross_out.at[b, e]
-        return copy(src, cross_in.at[b, e], x_send.at[b, e], x_recv.at[b, e], {"tp": far})
+        return copy(src, cross_in.at[b, e], x_send.at[0], x_recv.at[b, e], {"tp": far})
 
     def out_copy(b, e):
         to = s if e == 0 else edge
-        return copy(block_out.at[b, e], block_in.at[to], o_send.at[b, e], o_recv.at[to], {"sp": b})
+        return copy(block_out.at[b, e], block_in.at[to], o_send.at[0], o_recv.at[to], {"sp": b})
 
     def out_arrival(i):
-        return copy(block_out.at[0, 0], block_in.at[i], o_send.at[0, 0], o_recv.at[i], {"sp": near})
+        return copy(block_out.at[0, 0], block_in.at[i], o_send.at[0], o_recv.at[i], {"sp": near})
 
     def pool_copy(b):
         dst = pool_in.at[half]
         where = {"sp": b}
-        return copy(block_out.at[b, 0], dst, o_send.at[b, 0], o_recv.at[count + half], where)
+        return copy(block_out.at[b, 0], dst, o_send.at[0], o_recv.at[count + half], where)
 
     def pool_arrival(i):
         dst = pool_in.at[i]
-        return copy(block_out.at[0, 0], dst, o_send.at[0, 0], o_recv.at[count + i], {"sp": near})
+        return copy(block_out.at[0, 0], dst, o_send.at[0], o_recv.at[count + i], {"sp": near})
 
     local[0].wait()
     local[1].wait()
@@ -478,17 +524,18 @@
 
     local[2].wait()
     local[3].wait()
+    local[11].wait()
 
     sends_near = jnp.logical_not(inner) & (c == half)
-    sends_past = sends_on & jnp.logical_not(sends_near)
-
-    @pl.when(sends_near)
-    def _():
-        kv_first_whole().start()
-        for core in range(2):
-            q_whole(core).start()
-
-    @pl.when(sends_past)
+
+    sends_relay = jnp.logical_not(inner) & (c != half)
+
+    @pl.when(sends_relay)
+    def _():
+        for i in range(3):
+            relay_copy(i).start()
+
+    @pl.when(away)
     def _():
         kv_first().start()
         for core in range(2):
@@ -540,13 +587,23 @@
             send().start()
 
     def outer_work():
-        w_copy().start()
         with scope("otok"):
-            for owner in (near, count - 1 - near, far_edge):
-                z_copy(2 * owner, near).wait_recv()
-                z_copy(2 * owner + 1, near).wait_recv()
+            for u in (2 * near, 2 * near + 1, 2 * (count - 1 - near)):
+                z_copy(u, near).wait_recv()
+
+            @pl.when(sends_near)
+            def _():
+                kv_first_whole().start()
+                for core in range(2):
+                    q_whole(core).start()
+
+            z_copy(2 * (count - 1 - near) + 1, near).wait_recv()
+            z_copy(2 * far_edge, near).wait_recv()
+            z_copy(2 * far_edge + 1, near).wait_recv()
         with scope("opool"):
             lax.fori_loop(0, count, pool, 0)
+        w_copy(0).start()
+        w_copy(1).start()
         local[7].wait()
 
         def outer_steps(m, carry):
@@ -585,18 +642,18 @@
         def _():
             par_copy().start()
 
-        def tok_in(u, onward):
+        def tok_in(u, onward, beside=tok_forward):
             z_copy(u, other).wait_recv()
             if onward:
                 z_copy(u, other).start()
             else:
                 z_outward(u).start()
             tok_forward(1, u).start()
-            tok_forward(0, u).start()
-
-        def tok_x(u):
+            beside(0, u).start()
+
+        def tok_x(u, beside=tok_forward):
             tok_forward(1, u).wait_recv()
-            tok_forward(2, u).start()
+            beside(2, u).start()
 
         def kv_in(owner):
             @pl.when(at_home)
@@ -604,6 +661,10 @@
                 kv_arrival(owner, g).wait_recv()
                 kv_forward(0, owner).start()
                 kv_forward(1, owner).start()
+
+        def r_arrive(i):
+            relay_copy(i).wait_recv()
+            relay_forward(i).start()
 
         def kv_y(owner):
             @pl.when(at_home)
@@ -623,8 +684,35 @@
         with scope("tok1"):
             tok_in(2 * edge + 1, True)
             tok_in(2 * other + 1, False)
+        with scope("relay0"):
+
+            @pl.when(away)
+            def _():
+                r_arrive(0)
+
         with scope("kv1"):
             kv_in(other)
+        with scope("x0"):
+            tok_x(2 * edge)
+            tok_x(2 * other)
+        with scope("q1"):
+            q_in(other)
+        with scope("relay1"):
+
+            @pl.when(away)
+            def _():
+                r_arrive(1)
+                r_arrive(2)
+
+        with scope("tok2"):
+            tok_in(2 * far_edge, False, tok_late)
+        with scope("kvy1"):
+            kv_y(other)
+        with scope("x1"):
+            tok_x(2 * edge + 1)
+            tok_x(2 * other + 1)
+        with scope("tok3"):
+            tok_in(2 * far_edge + 1, False, tok_late)
         with scope("kv0"):
 
             @pl.when(at_home)
@@ -632,34 +720,44 @@
                 kv_edge().wait_recv()
                 kv_edge().start()
 
-        with scope("q1"):
-            q_in(other)
-        with scope("kvy1"):
-            kv_y(other)
-        with scope("tok2"):
-            tok_in(2 * far_edge, False)
-            tok_in(2 * far_edge + 1, False)
-        with scope("x01"):
-            for u in (2 * edge, 2 * other, 2 * edge + 1, 2 * other + 1):
-                tok_x(u)
         with scope("kv2"):
             kv_in(far_edge)
+        with scope("pool"):
+            lax.fori_loop(0, count, pool, 0)
         with scope("q2"):
             q_in(far_edge)
-        with scope("pool"):
-            lax.fori_loop(0, count, pool, 0)
         with scope("x2"):
-            tok_x(2 * far_edge)
-            tok_x(2 * far_edge + 1)
+            tok_x(2 * far_edge, tok_late)
+            tok_x(2 * far_edge + 1, tok_late)
         with scope("kvy2"):
             kv_y(far_edge)
-        with scope("rest"):
-            for owner in owners:
-                for u in (2 * owner, 2 * owner + 1):
-                    tok_forward(0, u).wait_recv()
-                    tok_forward(2, u).wait_recv()
-
-        with scope("kvrest"):
+
+        early = pl.ds(pl.multiple_of(half * rows, rows), 3 * rows)
+        late = span(far_edge, rows)
+        k_early = pl.ds(pl.multiple_of(half * shard, shard), 3 * shard)
+        k_late = span(far_edge, shard)
+
+        def early_product(store, w):
+            store[...] = jnp.dot(
+                norm_all[early, k_early], w[k_early, :], preferred_element_type=f32
+            )
+
+        def late_product(store, w, put):
+            acc = store[...] + jnp.dot(
+                norm_all[early, k_late], w[k_late, :], preferred_element_type=f32
+            )
+            put(early, acc.astype(bf16))
+            acc = jnp.dot(norm_all[late, :], w[...], preferred_element_type=f32)
+            put(late, acc.astype(bf16))
+
+        def early_tokens(step):
+            place = norm_all.at[0 : 2 * rows, 0:quarter]
+            got = f_recv.at[2 * count + step // 2]
+            return copy(place, place, f_send.at[step], got, {"tp": sib})
+
+        with scope("earlykv"):
+            for step in (0, 2):
+                early_tokens(step).wait_recv()
 
             @pl.when(at_home)
             def _():
@@ -670,34 +768,41 @@
             @pl.when(away)
             def _():
                 kv_edge().wait_recv()
-                for owner in split:
-                    kv_arrival(owner, g).wait_recv()
-                    kv_arrival(owner, twin).wait_recv()
+                kv_arrival(other, g).wait_recv()
+                kv_arrival(other, twin).wait_recv()
                 kv_beside().wait_recv()
                 q_beside().wait_recv()
                 par_copy().wait_recv()
 
-        def project_kv(b, carry):
-            acc = jnp.dot(norm_all[span(b, rows), :], w_kv[...], preferred_element_type=f32)
-            k_all[span(b, rows), :] = acc[:, 0:LANES].astype(bf16)
-            v_all[span(b, rows), :] = acc[:, LANES:pair].astype(bf16)
-            return carry
+            early_product(acc_kv, w_kv)
+        with scope("rest"):
+            for step in (0, 2):
+                for u in (2 * far_edge, 2 * far_edge + 1):
+                    tok_late(step, u).wait_recv()
+        with scope("kvrest"):
+
+            @pl.when(away)
+            def _():
+                kv_arrival(far_edge, g).wait_recv()
+                kv_arrival(far_edge, twin).wait_recv()
+
+        def put_kv(at, value):
+            k_all[at, :] = value[:, 0:LANES]
+            v_all[at, :] = value[:, LANES:pair]
+
+        def put_q(at, value):
+            q_all[at, :] = value
 
         with scope("projkv"):
-            lax.fori_loop(0, count, project_kv, 0)
-
+            late_product(acc_kv, w_kv, put_kv)
+        with scope("earlyq"):
+            q_edge().wait_recv()
+            q_arrival(other, twin).wait_recv()
+            early_product(acc_q, w_q)
         with scope("qrest"):
-            q_edge().wait_recv()
-            for owner in split:
-                q_arrival(owner, twin).wait_recv()
-
-        def project_q(b, carry):
-            acc = jnp.dot(norm_all[span(b, rows), :], w_q[...], preferred_element_type=f32)
-            q_all[span(b, rows), :] = acc.astype(bf16)
-            return carry
-
+            q_arrival(far_edge, twin).wait_recv()
         with scope("projq"):
-            lax.fori_loop(0, count, project_q, 0)
+            late_product(acc_q, w_q, put_q)
 
         par_use[...] = jnp.where(at_home, par_own[...], par_in[...])
         lane = lax.broadcasted_iota(jnp.int32, (rows, LANES), 1)
@@ -765,44 +870,47 @@
 
                     @pl.when(b == 0)
                     def _():
-                        w_copy().wait_recv()
-
-                total = jnp.dot(
-                    heads_all[span(b, rows), :], wa_all[e], preferred_element_type=f32
-                )
+                        with scope("wrest"):
+                            w_arrival(1).wait_recv()
+                            w_arrival(2).wait_recv()
+
+                total = jnp.dot(heads_all[span(b, rows), :], wa_all[e], preferred_element_type=f32)
                 hand_parts(b, e, total + pool_product(b) if e == 0 else total)
+
+        def attend_all(b, carry):
+            with scope("att"):
+                attend(b)
+
+            @pl.when(b == 0)
+            def _():
+                with scope("wao"):
+                    w_arrival(0).wait_recv()
+                    w_forward().start()
+
+            return carry
+
+        lax.fori_loop(0, count, attend_all, 0)
+        local[6].wait()
+        local[7].wait()
 
         def steps(m, carry):
             @pl.when(m < count)
             def _():
-                with scope("att"):
-                    attend(m)
-
-            @pl.when(m == 2)
-            def _():
-                local[6].wait()
-                local[7].wait()
-
-            @pl.when((m >= 3) & (m < count + 3))
-            def _():
+                with scope("S1"):
+                    first_sum(m)
                 with scope("S2"):
                     for e in range(2):
-                        second_sum(m - 3, e)
-
-            @pl.when((m >= 2) & (m < count + 2))
-            def _():
-                with scope("S1"):
-                    first_sum(m - 2)
-
-            @pl.when(m >= 4)
+                        second_sum(m, e)
+
+            @pl.when(m >= 2)
             def _():
                 with scope("S3"):
                     for e in range(2):
-                        third_sum(m - 4, e, lambda: out_copy(m - 4, e))
+                        third_sum(m - 2, e, lambda: out_copy(m - 2, e))
 
             return carry
 
-        lax.fori_loop(0, 2 * count, steps, 0)
+        lax.fori_loop(0, count + 2, steps, 0)
 
     pl.when(inner)(inner_work)
 
@@ -855,80 +963,57 @@
     @pl.when(sends_near)
     def _():
         kv_first_whole().wait_send()
-        for core in range(2):
-            q_whole(core).wait_send()
-
-    @pl.when(sends_past)
-    def _():
-        kv_first().wait_send()
-        for core in range(2):
-            q_copy(core).wait_send()
+        all_sent(w_q.at[0 : 2 * shard, :], q_send.at[0])
+
+    @pl.when(sends_relay | away)
+    def _():
+        relay_copy(0).wait_send()
+        all_sent(w_q.at[0:shard, :], q_send.at[0])
+
+    @pl.when(away)
+    def _():
+        relay_forward(0).wait_send()
+        all_sent(w_q.at[0:shard, :], q_send.at[2])
 
     @pl.when(jnp.logical_not(inner))
     def _():
-        z_copy(2 * s, near).wait_send()
-        z_copy(2 * s + 1, near).wait_send()
-        w_copy().wait_send()
-
-        def drain_outer(b, carry):
-            part_copy(b, 0).wait_send()
-            cross_copy(b, 0).wait_send()
-
-            @pl.when(b != s)
-            def _():
-                pool_copy(b).wait_send()
-
-            return carry
-
-        lax.fori_loop(0, count, drain_outer, 0)
+        all_sent(norm_all.at[0:rows, 0:quarter], z_send.at[0])
+        w_copy(0).wait_send()
+        w_copy(1).wait_send()
+        all_sent(part_in.at[:, 0], p_send.at[0])
+        all_sent(cross_in.at[:, 0], x_send.at[0])
+        all_sent(block_out.at[0 : count - 1, 0], o_send.at[0])
 
     @pl.when(at_home)
     def _():
         kv_beside().wait_send()
         q_beside().wait_send()
         par_copy().wait_send()
-        kv_edge().wait_send()
-        for owner in (other, far_edge):
-            for kind in range(3):
-                kv_forward(kind, owner).wait_send()
+        all_sent(w_kv, kv_fwd.at[0])
+
+    @pl.when(away)
+    def _():
+        all_sent(head_own, h_send.at[1])
 
     @pl.when(inner)
     def _():
-        for owner in (s, edge):
-            z_copy(2 * owner, other).wait_send()
-            z_copy(2 * owner + 1, other).wait_send()
-        for owner in (s, other, far_edge):
-            z_outward(2 * owner).wait_send()
-            z_outward(2 * owner + 1).wait_send()
-        for owner in (edge, other, far_edge):
-            for step in range(3):
-                tok_forward(step, 2 * owner).wait_send()
-                tok_forward(step, 2 * owner + 1).wait_send()
-        for owner in (other, far_edge):
-            q_forward(owner).wait_send()
-
-        def drain(b, carry):
-            head_copy(0, b).wait_send()
-
-            @pl.when(away)
-            def _():
-                head_copy(1, b).wait_send()
-
-            for h in range(2):
-                part_copy(b, h).wait_send()
-                cross_copy(b, h).wait_send()
-
-                @pl.when(b != s)
-                def _():
-                    out_copy(b, h).wait_send()
-
-            @pl.when(jnp.logical_not(at_home & (b == s)))
-            def _():
-                lt_copy(b).wait_send()
-
-            return carry
-
-        lax.fori_loop(0, count, drain, 0)
+        all_sent(norm_all.at[0 : 2 * rows, 0:quarter], z_send.at[0])
+        for sem in (z_send.at[1], f_send.at[0], f_send.at[1], f_send.at[2]):
+            all_sent(norm_all.at[0 : 3 * rows, 0:quarter], sem)
+        all_sent(w_q.at[0:shard, :], q_twin.at[0])
+        w_forward().wait_send()
+        all_sent(head_own, h_send.at[0])
+        all_sent(part_in, p_send.at[0])
+        all_sent(cross_in, x_send.at[0])
+        all_sent(block_out.at[0 : count - 1], o_send.at[0])
+
+    @pl.when(inner & jnp.logical_not(at_home))
+    def _():
+        all_sent(lt_send, l_send.at[0])
+
+    @pl.when(at_home)
+    def _():
+        all_sent(lt_send.at[0 : count - 1], l_send.at[0])
 
 
 def fused(
@@ -969,6 +1054,9 @@
             pltpu.VMEM((count, LANES), f32),
             pltpu.VMEM((seq, width), bf16),
             pltpu.VMEM((shard, pair), bf16),
+            pltpu.VMEM((shard, count * LANES), bf16),
+            pltpu.VMEM((shard // 2, pair), bf16),
+            pltpu.VMEM((2, shard // 2, pair), bf16),
             pltpu.VMEM((width, pair), bf16),
             pltpu.VMEM((width, pair), bf16),
             pltpu.VMEM((2, group, cols), bf16),
@@ -976,6 +1064,8 @@
             pltpu.VMEM((2 * count, LANES), f32),
             pltpu.VMEM((2 * count, LANES), f32),
             pltpu.VMEM((2 * count, LANES), f32),
+            pltpu.VMEM((3 * rows, pair), f32),
+            pltpu.VMEM((3 * rows, pair), f32),
             pltpu.VMEM((seq, pair), bf16),
             pltpu.VMEM((seq, LANES), bf16),
             pltpu.VMEM((seq, LANES), bf16),
@@ -991,30 +1081,31 @@
             pltpu.VMEM((2, sub, cols), bf16),
             pltpu.VMEM((count, 8, lt_rows), f32),
             pltpu.VMEM((2, 8, lt_rows), f32),
-            sems((11,)),
+            sems((12,)),
+            sems((2,)),
             sems((2 * count,)),
-            sems((2 * count,)),
-            sems((2 * count,)),
-            sems((3, 2 * count)),
-            sems((3, 2 * count)),
-            sems((2,)),
-            sems((3, count)),
+            sems((3,)),
+            sems((2 * count + 6,)),
+            sems((3,)),
+            sems((1,)),
             sems((count, 2)),
             sems((3,)),
-            sems((count,)),
+            sems((1,)),
+            sems((count, 2)),
+            sems((3,)),
+            sems((2,)),
+            sems((1,)),
+            sems((3,)),
+            sems((2,)),
+            sems((2,)),
             sems((count, 2)),
             sems((1,)),
+            sems((count, 2)),
             sems((1,)),
-            sems((2,)),
-            sems((2, count)),
             sems((count, 2)),
-            sems((count, 2)),
-            sems((count, 2)),
-            sems((count, 2)),
-            sems((count, 2)),
-            sems((count, 2)),
+            sems((1,)),
             sems((count + 2,)),
-            sems((count,)),
+            sems((1,)),
             sems((2,)),
         ],
         compiler_params=pltpu.CompilerParams(collective_id=0, has_side_effects=True),

time: 53.8 us -> 49.1 us (0.913)
  Pallas kernels: 51.7 us -> 47 us
    pallas_call x1, Pallas kernels: 51.7 us -> 47 us  [fused(): pl.pallas_call(functools.partial(fused_kernel, count), out_shape=(pltpu.V...]
where the time goes in v4:
time: 49.1 us; the launch traced here: 48.9 us
  Pallas kernels  47 us (96%)
  local copies, waits for them, and re-layouts  1.27 us (3%)
  between operations  0.64 us (1%)
    pallas_call x1, Pallas kernels, fused(): pl.pallas_call(functools.partial(fused_kernel, count), out_shape=(pltpu.V...  47 us
    unnamed x2, local copies, waits for them, and re-layouts  1.27 us

profile of v4, /device:TPU:24, one launch (start us, length us, event | category | flops | bytes accessed | tf_op | source)
XLA Modules:
  0.0 48.9 jit_solution(16488189042079080248)
XLA Ops:
  0.6 47.0 %shard_map.104 = (bf16[40,2048]{1,0:T(8,128)(2,1)S(1)}, f32[2,4,160]{2,1,0:T(4,128)S(1)}) custom-call(bf16[160,2048]{1,0:T(8,128)(2,1)} %tok.1, f32[1,2048]{1,0:T(1,128)} %bitcast.1, bf16[512,512]{1,0:T(8,128)(2,1)} %wq.1, bf16[512,128]{1,0:T(8,128)(2,1)} %wk.1, bf16[512,128]{1,0:T(8,128)(2,1)} %wv.1, f32[4]{0:T(128)} %lam.1, f32[4,128]{1,0:T(4,128)} %hgain.1, ...), custom_call_target="tpu_custom_call" | custom-call | tf_op jit(solution)/shard_map/pallas_call | solution.py:1042
  47.6 0.7 %copy.13 = bf16[40,2048]{1,0:T(8,128)(2,1)} copy(bf16[40,2048]{1,0:T(8,128)(2,1)S(1)} %get-tuple-element.2) | data formatting | bytes 327680
  48.3 0.6 %copy.14 = f32[2,4,160]{2,1,0:T(4,128)} copy(f32[2,4,160]{2,1,0:T(4,128)S(1)} %get-tuple-element.3) | data formatting | bytes 10240

commit v5 on v4

--- a/solution.py
+++ b/solution.py
@@ -187,6 +187,7 @@
     q_own,
     kv_relay,
     q_relay,
+    q_relay_whole,
     w_kv,
     w_q,
     wa_all,
@@ -407,9 +408,10 @@
     def relay_copy(i):
         if i == 0:
             src, dst = kv_own.at[span(g, part), :], kv_relay
+        elif i == 1:
+            src, dst = q_own.at[span(g, part), 0:pair], q_relay
         else:
-            src = q_own.at[span(g, part), (i - 1) * pair : i * pair]
-            dst = q_relay.at[i - 1]
+            src, dst = q_own.at[:, pair : 2 * pair], q_relay_whole
         send = kv_send.at[0] if i == 0 else q_send.at[0]
         return copy(src, dst, send, r_recv.at[i], {"sp": near})
 
@@ -417,9 +419,16 @@
         if i == 0:
             dst = w_kv.at[half_rows(edge, g), :]
             return copy(kv_relay, dst, kv_send.at[2], kv_recv.at[edge, g], {"sp": other})
-        dst = w_q.at[half_rows(edge, g), :]
         where = {"sp": other, "tp": 2 * x + i - 1}
-        return copy(q_relay.at[i - 1], dst, q_send.at[2], q_recv.at[edge, g], where)
+        if i == 1:
+            dst = w_q.at[half_rows(edge, g), :]
+            return copy(q_relay, dst, q_send.at[2], q_recv.at[edge, g], where)
+        dst = w_q.at[span(edge, shard), :]
+        return copy(q_relay_whole, dst, q_send.at[2], q_recv.at[edge, 0], where)
+
+    def q_far_whole():
+        place = w_q.at[span(far_edge, shard), :]
+        return copy(place, place, q_twin.at[0], q_recv.at[far_edge, 0], {"tp": sib})
 
     def q_beside():
         src = q_own.at[:, span(1 - c, pair)]
@@ -453,12 +462,12 @@
     head_where = ({"sp": other, "tp": home}, {"tp": sib})
 
     def head_copy(kind, b):
-        dst = heads_all.at[span(b, rows), span(c, pair)]
+        dst = heads_all.at[c, span(b, rows), :]
         src = head_own.at[span(b, rows), :]
         return copy(src, dst, h_send.at[kind], h_recv.at[b, c], head_where[kind])
 
     def head_arrival(b, core):
-        place = heads_all.at[span(b, rows), core * pair : (core + 1) * pair]
+        place = heads_all.at[core, span(b, rows), :]
         return copy(place, place, h_send.at[0], h_recv.at[b, core], {"tp": sib})
 
     def lt_copy(b):
@@ -596,14 +605,20 @@
                 kv_first_whole().start()
                 for core in range(2):
                     q_whole(core).start()
+                w_copy(0).start()
+                w_copy(1).start()
 
             z_copy(2 * (count - 1 - near) + 1, near).wait_recv()
             z_copy(2 * far_edge, near).wait_recv()
             z_copy(2 * far_edge + 1, near).wait_recv()
         with scope("opool"):
             lax.fori_loop(0, count, pool, 0)
-        w_copy(0).start()
-        w_copy(1).start()
+
+        @pl.when(sends_relay)
+        def _():
+            w_copy(0).start()
+            w_copy(1).start()
+
         local[7].wait()
 
         def outer_steps(m, carry):
@@ -702,7 +717,6 @@
             @pl.when(away)
             def _():
                 r_arrive(1)
-                r_arrive(2)
 
         with scope("tok2"):
             tok_in(2 * far_edge, False, tok_late)
@@ -713,6 +727,12 @@
             tok_x(2 * other + 1)
         with scope("tok3"):
             tok_in(2 * far_edge + 1, False, tok_late)
+        with scope("relay2"):
+
+            @pl.when(away)
+            def _():
+                r_arrive(2)
+
         with scope("kv0"):
 
             @pl.when(at_home)
@@ -725,12 +745,14 @@
         with scope("pool"):
             lax.fori_loop(0, count, pool, 0)
         with scope("q2"):
-            q_in(far_edge)
+
+            @pl.when(c == 0)
+            def _():
+                q_in(far_edge)
+
         with scope("x2"):
             tok_x(2 * far_edge, tok_late)
             tok_x(2 * far_edge + 1, tok_late)
-        with scope("kvy2"):
-            kv_y(far_edge)
 
         early = pl.ds(pl.multiple_of(half * rows, rows), 3 * rows)
         late = span(far_edge, rows)
@@ -775,6 +797,12 @@
                 par_copy().wait_recv()
 
             early_product(acc_kv, w_kv)
+        with scope("kvy2"):
+            kv_y(far_edge)
+        with scope("earlyq"):
+            q_edge().wait_recv()
+            q_arrival(other, twin).wait_recv()
+            early_product(acc_q, w_q)
         with scope("rest"):
             for step in (0, 2):
                 for u in (2 * far_edge, 2 * far_edge + 1):
@@ -795,12 +823,16 @@
 
         with scope("projkv"):
             late_product(acc_kv, w_kv, put_kv)
-        with scope("earlyq"):
-            q_edge().wait_recv()
-            q_arrival(other, twin).wait_recv()
-            early_product(acc_q, w_q)
         with scope("qrest"):
-            q_arrival(far_edge, twin).wait_recv()
+
+            @pl.when(c == 0)
+            def _():
+                q_arrival(far_edge, twin).wait_recv()
+
+            @pl.when(c == 1)
+            def _():
+                q_far_whole().wait_recv()
+
         with scope("projq"):
             late_product(acc_q, w_q, put_q)
 
@@ -844,7 +876,7 @@
 
             @pl.when(at_home)
             def _():
-                heads_all[span(b, rows), span(c, pair)] = head_own[span(b, rows), :]
+                heads_all[c, span(b, rows), :] = head_own[span(b, rows), :]
 
             both = jnp.where(
                 lane < 2,
@@ -874,14 +906,24 @@
                             w_arrival(1).wait_recv()
                             w_arrival(2).wait_recv()
 
-                total = jnp.dot(heads_all[span(b, rows), :], wa_all[e], preferred_element_type=f32)
+                total = sum(
+                    jnp.dot(
+                        heads_all[core, span(b, rows), :],
+                        wa_all[e, core * pair : (core + 1) * pair, :],
+                        preferred_element_type=f32,
+                    )
+                    for core in range(2)
+                )
                 hand_parts(b, e, total + pool_product(b) if e == 0 else total)
 
-        def attend_all(b, carry):
+        def nth(m):
+            return jnp.where(m < 2, (count - 1) * m, m - 1)
+
+        def attend_all(m, carry):
             with scope("att"):
-                attend(b)
-
-            @pl.when(b == 0)
+                attend(nth(m))
+
+            @pl.when(m == 0)
             def _():
                 with scope("wao"):
                     w_arrival(0).wait_recv()
@@ -897,16 +939,16 @@
             @pl.when(m < count)
             def _():
                 with scope("S1"):
-                    first_sum(m)
+                    first_sum(nth(m))
                 with scope("S2"):
                     for e in range(2):
-                        second_sum(m, e)
+                        second_sum(nth(m), e)
 
             @pl.when(m >= 2)
             def _():
                 with scope("S3"):
                     for e in range(2):
-                        third_sum(m - 2, e, lambda: out_copy(m - 2, e))
+                        third_sum(nth(m - 2), e, lambda: out_copy(nth(m - 2), e))
 
             return carry
 
@@ -965,15 +1007,17 @@
         kv_first_whole().wait_send()
         all_sent(w_q.at[0 : 2 * shard, :], q_send.at[0])
 
-    @pl.when(sends_relay | away)
+    @pl.when(sends_relay)
     def _():
         relay_copy(0).wait_send()
+        all_sent(w_q.at[0 : shard + part, :], q_send.at[0])
+
+    @pl.when(away)
+    def _():
+        kv_first().wait_send()
         all_sent(w_q.at[0:shard, :], q_send.at[0])
-
-    @pl.when(away)
-    def _():
         relay_forward(0).wait_send()
-        all_sent(w_q.at[0:shard, :], q_send.at[2])
+        all_sent(w_q.at[0 : shard + part, :], q_send.at[2])
 
     @pl.when(jnp.logical_not(inner))
     def _():
@@ -1000,7 +1044,15 @@
         all_sent(norm_all.at[0 : 2 * rows, 0:quarter], z_send.at[0])
         for sem in (z_send.at[1], f_send.at[0], f_send.at[1], f_send.at[2]):
             all_sent(norm_all.at[0 : 3 * rows, 0:quarter], sem)
-        all_sent(w_q.at[0:shard, :], q_twin.at[0])
+
+        @pl.when(c == 0)
+        def _():
+            all_sent(w_q.at[0:shard, :], q_twin.at[0])
+
+        @pl.when(c == 1)
+        def _():
+            all_sent(w_q.at[0:part, :], q_twin.at[0])
+
         w_forward().wait_send()
         all_sent(head_own, h_send.at[0])
         all_sent(part_in, p_send.at[0])
@@ -1056,7 +1108,8 @@
             pltpu.VMEM((shard, pair), bf16),
             pltpu.VMEM((shard, count * LANES), bf16),
             pltpu.VMEM((shard // 2, pair), bf16),
-            pltpu.VMEM((2, shard // 2, pair), bf16),
+            pltpu.VMEM((shard // 2, pair), bf16),
+            pltpu.VMEM((shard, pair), bf16),
             pltpu.VMEM((width, pair), bf16),
             pltpu.VMEM((width, pair), bf16),
             pltpu.VMEM((2, group, cols), bf16),
@@ -1070,7 +1123,7 @@
             pltpu.VMEM((seq, LANES), bf16),
             pltpu.VMEM((seq, LANES), bf16),
             pltpu.VMEM((seq, pair), bf16),
-            pltpu.VMEM((seq, count * LANES), bf16),
+            pltpu.VMEM((2, seq, pair), bf16),
             pltpu.VMEM((seq, group), bf16),
             pltpu.VMEM((count, 2, 2, 2, sub, cols), bf16),
             pltpu.VMEM((count, 2, 2, sub, cols), bf16),

time: 49.1 us -> 47.4 us (0.965)
  the two profiles are of different devices: /device:TPU:24 before, /device:TPU:16 now
where the time goes in v5:
time: 47.4 us; the launch traced here: 47.2 us
  Pallas kernels  45.3 us (96%)
  local copies, waits for them, and re-layouts  1.27 us (3%)
  between operations  0.64 us (1%)
    pallas_call x1, Pallas kernels, fused(): pl.pallas_call(functools.partial(fused_kernel, count), out_shape=(pltpu.V...  45.3 us
    unnamed x2, local copies, waits for them, and re-layouts  1.27 us

profile of v5, /device:TPU:16, one launch (start us, length us, event | category | flops | bytes accessed | tf_op | source)
XLA Modules:
  0.0 47.2 jit_solution(12722054600889725021)
XLA Ops:
  0.6 45.3 %shard_map.104 = (bf16[40,2048]{1,0:T(8,128)(2,1)S(1)}, f32[2,4,160]{2,1,0:T(4,128)S(1)}) custom-call(bf16[160,2048]{1,0:T(8,128)(2,1)} %tok.1, f32[1,2048]{1,0:T(1,128)} %bitcast.1, bf16[512,512]{1,0:T(8,128)(2,1)} %wq.1, bf16[512,128]{1,0:T(8,128)(2,1)} %wk.1, bf16[512,128]{1,0:T(8,128)(2,1)} %wv.1, f32[4]{0:T(128)} %lam.1, f32[4,128]{1,0:T(4,128)} %hgain.1, ...), custom_call_target="tpu_custom_call" | custom-call | tf_op jit(solution)/shard_map/pallas_call | solution.py:1094
  46.0 0.7 %copy.13 = bf16[40,2048]{1,0:T(8,128)(2,1)} copy(bf16[40,2048]{1,0:T(8,128)(2,1)S(1)} %get-tuple-element.2) | data formatting | bytes 327680
  46.6 0.6 %copy.14 = f32[2,4,160]{2,1,0:T(4,128)} copy(f32[2,4,160]{2,1,0:T(4,128)S(1)} %get-tuple-element.3) | data formatting | bytes 10240

commit v6 on v5

--- a/solution.py
+++ b/solution.py
@@ -611,33 +611,35 @@
             z_copy(2 * (count - 1 - near) + 1, near).wait_recv()
             z_copy(2 * far_edge, near).wait_recv()
             z_copy(2 * far_edge + 1, near).wait_recv()
+        local[7].wait()
+
+        def turn(m):
+            return jnp.where(half == 0, count - 1 - m, m)
+
+        def hand_on(m, carry):
+            pool(turn(m), 0)
+            hand_parts(turn(m), 0, pool_product(turn(m)))
+            return carry
+
         with scope("opool"):
-            lax.fori_loop(0, count, pool, 0)
+            lax.fori_loop(0, count, hand_on, 0)
 
         @pl.when(sends_relay)
         def _():
             w_copy(0).start()
             w_copy(1).start()
 
-        local[7].wait()
-
-        def outer_steps(m, carry):
-            @pl.when((m >= 1) & (m < count + 1))
-            def _():
-                second_sum(m - 1, 0)
-
-            @pl.when(m < count)
-            def _():
-                hand_parts(m, 0, pool_product(m))
-
-            @pl.when(m >= 2)
-            def _():
-                third_sum(m - 2, 0, lambda: pool_copy(m - 2))
-
+        def cross_over(m, carry):
+            second_sum(turn(m), 0)
             return carry
 
+        def hand_out(m, carry):
+            third_sum(turn(m), 0, lambda: pool_copy(turn(m)))
+            return carry
+
         with scope("osum"):
-            lax.fori_loop(0, count + 2, outer_steps, 0)
+            lax.fori_loop(0, count, cross_over, 0)
+            lax.fori_loop(0, count, hand_out, 0)
 
     pl.when(jnp.logical_not(inner))(outer_work)
 
@@ -841,31 +843,39 @@
         lt_rows = lt_send.shape[2]
         base = HD ** (-0.5)
 
-        def one_head(b, h):
-            head = 2 * c + h
-            q = q_all[span(b, rows), h * LANES : (h + 1) * LANES]
-            zero = jnp.zeros_like(q)
-            both_q = jnp.concatenate(
-                [jnp.where(lane < HD, q, zero), jnp.where(lane < HD, zero, q)], axis=0
-            )
+        def two_heads(b):
+            zero = jnp.zeros((rows, LANES), bf16)
+            parts = []
+            for h in range(2):
+                q = q_all[span(b, rows), h * LANES : (h + 1) * LANES]
+                parts += [jnp.where(lane < HD, q, zero), jnp.where(lane < HD, zero, q)]
             raw = lax.dot_general(
-                both_q, k_all[...], (((1,), (1,)), ((), ())), preferred_element_type=f32
+                jnp.concatenate(parts, axis=0),
+                k_all[...],
+                (((1,), (1,)), ((), ())),
+                preferred_element_type=f32,
             )
             highest = jnp.max(raw, axis=-1, keepdims=True)
             weights = jnp.exp2((raw - highest) * (base * math.log2(math.e)))
             totals = jnp.sum(weights, axis=-1, keepdims=True)
             reads = jnp.dot(weights.astype(bf16), v_all[...], preferred_element_type=f32) / totals
             logs = highest * base + jnp.log(totals)
-            contrast = reads[:rows] - par_use[pl.ds(count + head, 1), :] * reads[rows:]
-            scaled = (
-                contrast
-                * lax.rsqrt(jnp.mean(contrast * contrast, axis=-1, keepdims=True) + epsilon)
-                * par_use[pl.ds(head, 1), :]
-            ).astype(bf16)
-            return scaled, logs[:rows], logs[rows:]
+            done = []
+            for h in range(2):
+                head = 2 * c + h
+                first = slice(2 * h * rows, (2 * h + 1) * rows)
+                second = slice((2 * h + 1) * rows, (2 * h + 2) * rows)
+                contrast = reads[first] - par_use[pl.ds(count + head, 1), :] * reads[second]
+                scaled = (
+                    contrast
+                    * lax.rsqrt(jnp.mean(contrast * contrast, axis=-1, keepdims=True) + epsilon)
+                    * par_use[pl.ds(head, 1), :]
+                ).astype(bf16)
+                done.append((scaled, logs[first], logs[second]))
+            return done
 
         def attend(b):
-            done = [one_head(b, h) for h in range(2)]
+            done = two_heads(b)
             for h in range(2):
                 head_own[span(b, rows), h * LANES : (h + 1) * LANES] = done[h][0]
             head_copy(0, b).start()
@@ -886,35 +896,30 @@
             padded = jnp.concatenate([both, jnp.zeros((lt_rows - rows, LANES), f32)], axis=0)
             lt_send[b] = jnp.transpose(padded)[0:8, :]
 
+        def send_logs(b, carry):
             @pl.when(jnp.logical_not(at_home & (b == s)))
             def _():
                 lt_copy(b).start()
 
-        def first_sum(b):
-            for core in range(2):
-
-                @pl.when(jnp.logical_not(at_home & (c == core)))
-                def _():
-                    head_arrival(b, core).wait_recv()
-
-            for e in range(2):
-                if e == 1:
-
-                    @pl.when(b == 0)
+            return carry
+
+        def first_sum(b, e):
+            if e == 0:
+                for core in range(2):
+
+                    @pl.when(jnp.logical_not(at_home & (c == core)))
                     def _():
-                        with scope("wrest"):
-                            w_arrival(1).wait_recv()
-                            w_arrival(2).wait_recv()
-
-                total = sum(
-                    jnp.dot(
-                        heads_all[core, span(b, rows), :],
-                        wa_all[e, core * pair : (core + 1) * pair, :],
-                        preferred_element_type=f32,
-                    )
-                    for core in range(2)
+                        head_arrival(b, core).wait_recv()
+
+            total = sum(
+                jnp.dot(
+                    heads_all[core, span(b, rows), :],
+                    wa_all[e, core * pair : (core + 1) * pair, :],
+                    preferred_element_type=f32,
                 )
-                hand_parts(b, e, total + pool_product(b) if e == 0 else total)
+                for core in range(2)
+            )
+            hand_parts(b, e, total + pool_product(b) if e == 0 else total)
 
         def nth(m):
             return jnp.where(m < 2, (count - 1) * m, m - 1)
@@ -923,7 +928,7 @@
             with scope("att"):
                 attend(nth(m))
 
-            @pl.when(m == 0)
+            @pl.when(m == jnp.where(at_home, 0, 1))
             def _():
                 with scope("wao"):
                     w_arrival(0).wait_recv()
@@ -935,11 +940,23 @@
         local[6].wait()
         local[7].wait()
 
+        with scope("S1"):
+            first_sum(0, 0)
+        lax.fori_loop(0, count, send_logs, 0)
+        with scope("S2"):
+            second_sum(0, 0)
+        with scope("wrest"):
+            w_arrival(1).wait_recv()
+            w_arrival(2).wait_recv()
+        first_sum(0, 1)
+        second_sum(0, 1)
+
         def steps(m, carry):
             @pl.when(m < count)
             def _():
                 with scope("S1"):
-                    first_sum(nth(m))
+                    for e in range(2):
+                        first_sum(nth(m), e)
                 with scope("S2"):
                     for e in range(2):
                         second_sum(nth(m), e)
@@ -952,7 +969,7 @@
 
             return carry
 
-        lax.fori_loop(0, count + 2, steps, 0)
+        lax.fori_loop(1, count + 2, steps, 0)
 
     pl.when(inner)(inner_work)
 

time: 47.4 us -> 47 us (level)
  no operation moved by 1% of the time
where the time goes in v6:
time: 47 us; the launch traced here: 46.9 us
  Pallas kernels  44.9 us (96%)
  local copies, waits for them, and re-layouts  1.27 us (3%)
  between operations  0.64 us (1%)
    pallas_call x1, Pallas kernels, fused(): pl.pallas_call(functools.partial(fused_kernel, count), out_shape=(pltpu.V...  44.9 us
    unnamed x2, local copies, waits for them, and re-layouts  1.27 us

profile of v6, /device:TPU:16, one launch (start us, length us, event | category | flops | bytes accessed | tf_op | source)
XLA Modules:
  0.0 46.9 jit_solution(14226931191256311751)
XLA Ops:
  0.6 44.9 %shard_map.104 = (bf16[40,2048]{1,0:T(8,128)(2,1)S(1)}, f32[2,4,160]{2,1,0:T(4,128)S(1)}) custom-call(bf16[160,2048]{1,0:T(8,128)(2,1)} %tok.1, f32[1,2048]{1,0:T(1,128)} %bitcast.1, bf16[512,512]{1,0:T(8,128)(2,1)} %wq.1, bf16[512,128]{1,0:T(8,128)(2,1)} %wk.1, bf16[512,128]{1,0:T(8,128)(2,1)} %wv.1, f32[4]{0:T(128)} %lam.1, f32[4,128]{1,0:T(4,128)} %hgain.1, ...), custom_call_target="tpu_custom_call" | custom-call | tf_op jit(solution)/shard_map/pallas_call | solution.py:1111
  45.6 0.7 %copy.13 = bf16[40,2048]{1,0:T(8,128)(2,1)} copy(bf16[40,2048]{1,0:T(8,128)(2,1)S(1)} %get-tuple-element.2) | data formatting | bytes 327680
  46.3 0.6 %copy.14 = f32[2,4,160]{2,1,0:T(4,128)} copy(f32[2,4,160]{2,1,0:T(4,128)S(1)} %get-tuple-element.3) | data formatting | bytes 10240

commit v7 on v6

--- a/solution.py
+++ b/solution.py
@@ -215,20 +215,13 @@
     local_sem,
     z_send,
     z_recv,
-    f_send,
     f_recv,
     kv_send,
-    kv_fwd,
     kv_recv,
-    q_send,
-    q_twin,
     q_recv,
     r_recv,
-    w_send,
-    w_fwd,
     w_recv,
     par_sem,
-    h_send,
     h_recv,
     p_send,
     p_recv,
@@ -277,14 +270,18 @@
     def greet(where):
         pl.semaphore_signal(barrier, inc=1, device_id=where, device_id_type=MESH)
 
-    for off in range(1, count):
-        peer = lax.rem(s + off, count)
-        peer_inner = (peer > 0) & (peer < count - 1)
-
-        @pl.when(inner | peer_inner)
-        def _():
-            greet({"sp": peer})
-            greet({"sp": peer, "tp": sib})
+    def greet_beside(up):
+        peer = lax.rem(s + (1 if up else count - 1), count)
+        greet({"sp": peer})
+        greet({"sp": peer, "tp": sib})
+
+    @pl.when(s < count - 1)
+    def _():
+        greet_beside(True)
+
+    @pl.when(s > 0)
+    def _():
+        greet_beside(False)
 
     greet({"tp": sib})
     greet({"tp": far})
@@ -344,20 +341,20 @@
 
     def z_outward(u):
         place = norm_all.at[span(u, chunk), span(t, quarter)]
-        return copy(place, place, z_send.at[1], z_recv.at[u], {"sp": edge})
+        return copy(place, place, z_send.at[0], z_recv.at[u], {"sp": edge})
 
     def tok_forward(step, u):
         col = span(far if step == 2 else t, quarter)
         place = norm_all.at[span(u, chunk), col]
         where = {"tp": far if step == 1 else sib}
         got = f_recv.at[u] if step == 1 else f_recv.at[2 * count + step // 2]
-        return copy(place, place, f_send.at[step], got, where)
+        return copy(place, place, z_send.at[0], got, where)
 
     def tok_late(step, u):
         col = span(far if step == 2 else t, quarter)
         place = norm_all.at[span(u, chunk), col]
         got = f_recv.at[2 * count + 2 + step + lax.rem(u, 2)]
-        return copy(place, place, f_send.at[step], got, {"tp": sib})
+        return copy(place, place, z_send.at[0], got, {"tp": sib})
 
     def all_sent(ref, sem):
         copy(ref, ref, sem, sem, {"tp": sib}).wait_send()
@@ -373,37 +370,37 @@
 
     def kv_beside():
         dst = w_kv.at[span(s, shard), :]
-        return copy(kv_own, dst, kv_send.at[1], kv_recv.at[s, 0], {"tp": sib})
+        return copy(kv_own, dst, kv_send.at[0], kv_recv.at[s, 0], {"tp": sib})
 
     def kv_edge():
         place = w_kv.at[span(edge, shard), :]
-        return copy(place, place, kv_fwd.at[0], kv_recv.at[edge, 0], {"tp": sib})
+        return copy(place, place, kv_send.at[0], kv_recv.at[edge, 0], {"tp": sib})
 
     def kv_forward(kind, owner):
         which = twin if kind == 2 else g
         place = w_kv.at[half_rows(owner, which), :]
         where = {"grp": twin} if kind == 0 else {"tp": sib}
-        return copy(place, place, kv_fwd.at[0], kv_recv.at[owner, which], where)
+        return copy(place, place, kv_send.at[0], kv_recv.at[owner, which], where)
 
     def kv_arrival(owner, which):
         place = w_kv.at[half_rows(owner, which), :]
-        return copy(place, place, kv_fwd.at[0], kv_recv.at[owner, which], {"tp": sib})
+        return copy(place, place, kv_send.at[0], kv_recv.at[owner, which], {"tp": sib})
 
     def q_copy(core):
         src = q_own.at[span(g, part), core * pair : (core + 1) * pair]
         dst = w_q.at[half_rows(s, g), :]
         where = {"sp": target, "tp": 2 * x + core}
-        return copy(src, dst, q_send.at[0], q_recv.at[s, g], where)
+        return copy(src, dst, kv_send.at[0], q_recv.at[s, g], where)
 
     def q_whole(core):
         src = q_own.at[:, core * pair : (core + 1) * pair]
         dst = w_q.at[span(s, shard), :]
         where = {"sp": near, "tp": 2 * x + core}
-        return copy(src, dst, q_send.at[0], q_recv.at[s, 0], where)
+        return copy(src, dst, kv_send.at[0], q_recv.at[s, 0], where)
 
     def q_edge():
         place = w_q.at[span(edge, shard), :]
-        return copy(place, place, q_twin.at[0], q_recv.at[edge, 0], {"tp": sib})
+        return copy(place, place, kv_send.at[0], q_recv.at[edge, 0], {"tp": sib})
 
     def relay_copy(i):
         if i == 0:
@@ -412,49 +409,49 @@
             src, dst = q_own.at[span(g, part), 0:pair], q_relay
         else:
             src, dst = q_own.at[:, pair : 2 * pair], q_relay_whole
-        send = kv_send.at[0] if i == 0 else q_send.at[0]
+        send = kv_send.at[0]
         return copy(src, dst, send, r_recv.at[i], {"sp": near})
 
     def relay_forward(i):
         if i == 0:
             dst = w_kv.at[half_rows(edge, g), :]
-            return copy(kv_relay, dst, kv_send.at[2], kv_recv.at[edge, g], {"sp": other})
+            return copy(kv_relay, dst, kv_send.at[0], kv_recv.at[edge, g], {"sp": other})
         where = {"sp": other, "tp": 2 * x + i - 1}
         if i == 1:
             dst = w_q.at[half_rows(edge, g), :]
-            return copy(q_relay, dst, q_send.at[2], q_recv.at[edge, g], where)
+            return copy(q_relay, dst, kv_send.at[0], q_recv.at[edge, g], where)
         dst = w_q.at[span(edge, shard), :]
-        return copy(q_relay_whole, dst, q_send.at[2], q_recv.at[edge, 0], where)
+        return copy(q_relay_whole, dst, kv_send.at[0], q_recv.at[edge, 0], where)
 
     def q_far_whole():
         place = w_q.at[span(far_edge, shard), :]
-        return copy(place, place, q_twin.at[0], q_recv.at[far_edge, 0], {"tp": sib})
+        return copy(place, place, kv_send.at[0], q_recv.at[far_edge, 0], {"tp": sib})
 
     def q_beside():
         src = q_own.at[:, span(1 - c, pair)]
-        return copy(src, w_q.at[span(s, shard), :], q_send.at[1], q_recv.at[s, 0], {"tp": sib})
+        return copy(src, w_q.at[span(s, shard), :], kv_send.at[0], q_recv.at[s, 0], {"tp": sib})
 
     def q_forward(owner):
         place = w_q.at[half_rows(owner, g), :]
-        return copy(place, place, q_twin.at[0], q_recv.at[owner, g], {"grp": twin})
+        return copy(place, place, kv_send.at[0], q_recv.at[owner, g], {"grp": twin})
 
     def q_arrival(owner, which):
         place = w_q.at[half_rows(owner, which), :]
-        return copy(place, place, q_twin.at[0], q_recv.at[owner, which], {"grp": twin})
+        return copy(place, place, kv_send.at[0], q_recv.at[owner, which], {"grp": twin})
 
     w_rows = (span(g, part // 2), pl.ds(part, part), span(twin, part // 2))
 
     def w_copy(kind):
         src, dst = wao.at[w_rows[kind], :], wa_all.at[1, w_rows[kind], :]
-        return copy(src, dst, w_send.at[kind], w_recv.at[kind], {"sp": near})
+        return copy(src, dst, kv_send.at[0], w_recv.at[kind], {"sp": near})
 
     def w_forward():
         place = wa_all.at[1, w_rows[0], :]
-        return copy(place, place, w_fwd.at[0], w_recv.at[2], {"grp": twin})
+        return copy(place, place, kv_send.at[0], w_recv.at[2], {"grp": twin})
 
     def w_arrival(kind):
         place = wa_all.at[1, w_rows[kind], :]
-        return copy(place, place, w_fwd.at[0], w_recv.at[kind], {"grp": twin})
+        return copy(place, place, kv_send.at[0], w_recv.at[kind], {"grp": twin})
 
     def par_copy():
         return copy(par_own, par_in, par_sem.at[0], par_sem.at[1], {"tp": sib})
@@ -464,11 +461,11 @@
     def head_copy(kind, b):
         dst = heads_all.at[c, span(b, rows), :]
         src = head_own.at[span(b, rows), :]
-        return copy(src, dst, h_send.at[kind], h_recv.at[b, c], head_where[kind])
+        return copy(src, dst, kv_send.at[0], h_recv.at[b, c], head_where[kind])
 
     def head_arrival(b, core):
         place = heads_all.at[core, span(b, rows), :]
-        return copy(place, place, h_send.at[0], h_recv.at[b, core], {"tp": sib})
+        return copy(place, place, kv_send.at[0], h_recv.at[b, core], {"tp": sib})
 
     def lt_copy(b):
         where = {"sp": b, "tp": home}
@@ -516,7 +513,7 @@
     with scope("norm"):
         lax.fori_loop(0, rows // step, norm_rows, 0)
     with scope("barrier"):
-        pl.semaphore_wait(barrier, jnp.where(inner, 9, 6))
+        pl.semaphore_wait(barrier, jnp.where(inner, 7, 4))
     sends_on = s != target
 
     @pl.when(inner)
@@ -777,7 +774,7 @@
         def early_tokens(step):
             place = norm_all.at[0 : 2 * rows, 0:quarter]
             got = f_recv.at[2 * count + step // 2]
-            return copy(place, place, f_send.at[step], got, {"tp": sib})
+            return copy(place, place, z_send.at[0], got, {"tp": sib})
 
         with scope("earlykv"):
             for step in (0, 2):
@@ -1019,59 +1016,41 @@
                     both = mixed_out[:, at].astype(f32) + pool_in[which].astype(f32)
                     mixed_out[:, at] = both.astype(bf16)
 
+    def weights_sent(amount):
+        all_sent(norm_all.at[0 : amount * pair // width, :], kv_send.at[0])
+
     @pl.when(sends_near)
     def _():
-        kv_first_whole().wait_send()
-        all_sent(w_q.at[0 : 2 * shard, :], q_send.at[0])
+        weights_sent(3 * shard + 3 * part)
 
     @pl.when(sends_relay)
     def _():
-        relay_copy(0).wait_send()
-        all_sent(w_q.at[0 : shard + part, :], q_send.at[0])
-
-    @pl.when(away)
-    def _():
-        kv_first().wait_send()
-        all_sent(w_q.at[0:shard, :], q_send.at[0])
-        relay_forward(0).wait_send()
-        all_sent(w_q.at[0 : shard + part, :], q_send.at[2])
+        weights_sent(shard + 5 * part)
+
+    for core in range(2):
+
+        @pl.when(at_home & (c == core))
+        def _():
+            weights_sent(3 * shard + (9 - core) * part + seq)
+
+        @pl.when(away & (c == core))
+        def _():
+            weights_sent(shard + (8 - core) * part + 2 * seq)
 
     @pl.when(jnp.logical_not(inner))
     def _():
         all_sent(norm_all.at[0:rows, 0:quarter], z_send.at[0])
-        w_copy(0).wait_send()
-        w_copy(1).wait_send()
         all_sent(part_in.at[:, 0], p_send.at[0])
         all_sent(cross_in.at[:, 0], x_send.at[0])
         all_sent(block_out.at[0 : count - 1, 0], o_send.at[0])
 
     @pl.when(at_home)
     def _():
-        kv_beside().wait_send()
-        q_beside().wait_send()
         par_copy().wait_send()
-        all_sent(w_kv, kv_fwd.at[0])
-
-    @pl.when(away)
-    def _():
-        all_sent(head_own, h_send.at[1])
 
     @pl.when(inner)
     def _():
-        all_sent(norm_all.at[0 : 2 * rows, 0:quarter], z_send.at[0])
-        for sem in (z_send.at[1], f_send.at[0], f_send.at[1], f_send.at[2]):
-            all_sent(norm_all.at[0 : 3 * rows, 0:quarter], sem)
-
-        @pl.when(c == 0)
-        def _():
-            all_sent(w_q.at[0:shard, :], q_twin.at[0])
-
-        @pl.when(c == 1)
-        def _():
-            all_sent(w_q.at[0:part, :], q_twin.at[0])
-
-        w_forward().wait_send()
-        all_sent(head_own, h_send.at[0])
+        all_sent(norm_all.at[0 : 7 * rows // 2, :], z_send.at[0])
         all_sent(part_in, p_send.at[0])
         all_sent(cross_in, x_send.at[0])
         all_sent(block_out.at[0 : count - 1], o_send.at[0])
@@ -1152,21 +1131,14 @@
             pltpu.VMEM((count, 8, lt_rows), f32),
             pltpu.VMEM((2, 8, lt_rows), f32),
             sems((12,)),
-            sems((2,)),
+            sems((1,)),
             sems((2 * count,)),
-            sems((3,)),
             sems((2 * count + 6,)),
-            sems((3,)),
             sems((1,)),
             sems((count, 2)),
-            sems((3,)),
-            sems((1,)),
             sems((count, 2)),
             sems((3,)),
-            sems((2,)),
-            sems((1,)),
             sems((3,)),
-            sems((2,)),
             sems((2,)),
             sems((count, 2)),
             sems((1,)),

time: 47 us -> 46.6 us (level)
  no operation moved by 1% of the time
where the time goes in v7:
time: 46.6 us; the launch traced here: 46.4 us
  Pallas kernels  44.5 us (95%)
  local copies, waits for them, and re-layouts  1.27 us (3%)
  between operations  0.64 us (1%)
    pallas_call x1, Pallas kernels, fused(): pl.pallas_call(functools.partial(fused_kernel, count), out_shape=(pltpu.V...  44.5 us
    unnamed x2, local copies, waits for them, and re-layouts  1.27 us

profile of v7, /device:TPU:16, one launch (start us, length us, event | category | flops | bytes accessed | tf_op | source)
XLA Modules:
  0.0 46.4 jit_solution(6660280338616328171)
XLA Ops:
  0.6 44.5 %shard_map.104 = (bf16[40,2048]{1,0:T(8,128)(2,1)S(1)}, f32[2,4,160]{2,1,0:T(4,128)S(1)}) custom-call(bf16[160,2048]{1,0:T(8,128)(2,1)} %tok.1, f32[1,2048]{1,0:T(1,128)} %bitcast.1, bf16[512,512]{1,0:T(8,128)(2,1)} %wq.1, bf16[512,128]{1,0:T(8,128)(2,1)} %wk.1, bf16[512,128]{1,0:T(8,128)(2,1)} %wv.1, f32[4]{0:T(128)} %lam.1, f32[4,128]{1,0:T(4,128)} %hgain.1, ...), custom_call_target="tpu_custom_call" | custom-call | tf_op jit(solution)/shard_map/pallas_call | solution.py:1090
  45.1 0.7 %copy.13 = bf16[40,2048]{1,0:T(8,128)(2,1)} copy(bf16[40,2048]{1,0:T(8,128)(2,1)S(1)} %get-tuple-element.2) | data formatting | bytes 327680
  45.8 0.6 %copy.14 = f32[2,4,160]{2,1,0:T(4,128)} copy(f32[2,4,160]{2,1,0:T(4,128)S(1)} %get-tuple-element.3) | data formatting | bytes 10240

commit v8 on v7

--- a/solution.py
+++ b/solution.py
@@ -798,10 +798,27 @@
             early_product(acc_kv, w_kv)
         with scope("kvy2"):
             kv_y(far_edge)
+        k_edge = span(edge, shard)
+
+        def add_edge():
+            q_edge().wait_recv()
+            acc_q[...] += jnp.dot(
+                norm_all[early, k_edge], w_q[k_edge, :], preferred_element_type=f32
+            )
+
         with scope("earlyq"):
-            q_edge().wait_recv()
             q_arrival(other, twin).wait_recv()
-            early_product(acc_q, w_q)
+            acc_q[...] = jnp.dot(
+                norm_all[early, shard : 3 * shard],
+                w_q[shard : 3 * shard, :],
+                preferred_element_type=f32,
+            )
+
+        @pl.when(away)
+        def _():
+            with scope("edgeq"):
+                add_edge()
+
         with scope("rest"):
             for step in (0, 2):
                 for u in (2 * far_edge, 2 * far_edge + 1):
@@ -822,6 +839,11 @@
 
         with scope("projkv"):
             late_product(acc_kv, w_kv, put_kv)
+        @pl.when(at_home)
+        def _():
+            with scope("edgeq"):
+                add_edge()
+
         with scope("qrest"):
 
             @pl.when(c == 0)

time: 46.6 us -> 46.2 us (level)
  no operation moved by 1% of the time
where the time goes in v8:
time: 46.2 us; the launch traced here: 46.1 us
  Pallas kernels  44.2 us (96%)
  local copies, waits for them, and re-layouts  1.27 us (3%)
  between operations  0.64 us (1%)
    pallas_call x1, Pallas kernels, fused(): pl.pallas_call(functools.partial(fused_kernel, count), out_shape=(pltpu.V...  44.2 us
    unnamed x2, local copies, waits for them, and re-layouts  1.27 us

profile of v8, /device:TPU:16, one launch (start us, length us, event | category | flops | bytes accessed | tf_op | source)
XLA Modules:
  0.0 46.1 jit_solution(5605153154799985108)
XLA Ops:
  0.6 44.2 %shard_map.104 = (bf16[40,2048]{1,0:T(8,128)(2,1)S(1)}, f32[2,4,160]{2,1,0:T(4,128)S(1)}) custom-call(bf16[160,2048]{1,0:T(8,128)(2,1)} %tok.1, f32[1,2048]{1,0:T(1,128)} %bitcast.1, bf16[512,512]{1,0:T(8,128)(2,1)} %wq.1, bf16[512,128]{1,0:T(8,128)(2,1)} %wk.1, bf16[512,128]{1,0:T(8,128)(2,1)} %wv.1, f32[4]{0:T(128)} %lam.1, f32[4,128]{1,0:T(4,128)} %hgain.1, ...), custom_call_target="tpu_custom_call" | custom-call | tf_op jit(solution)/shard_map/pallas_call | solution.py:1112
  44.8 0.7 %copy.13 = bf16[40,2048]{1,0:T(8,128)(2,1)} copy(bf16[40,2048]{1,0:T(8,128)(2,1)S(1)} %get-tuple-element.2) | data formatting | bytes 327680
  45.5 0.6 %copy.14 = f32[2,4,160]{2,1,0:T(4,128)} copy(f32[2,4,160]{2,1,0:T(4,128)S(1)} %get-tuple-element.3) | data formatting | bytes 10240
